TPU v7x, 32 devices: a whole 2x2x4 slice. The times are simulated.
32 devices in a mesh: sp: 8 (over z, core), tp: 4 (over y, x).
Axes of the slice: x: 2, y: 2, z: 4, core: 2. Of those that a mesh axis runs over, the one named last changes fastest.
Arguments:
- query_heads: bfloat16 [2048, 1024], P('sp', 'tp'), may hold values from -6 to 6
- key_heads: bfloat16 [2048, 256], P('sp'), may hold values from -6 to 6
- value_heads: bfloat16 [2048, 256], P('sp'), may hold values from -24 to 24
- q_gain: float32 [64], replicated, may hold values from 0.6 to 4.5
- k_gain: float32 [64], replicated, may hold values from 0.6 to 4.5
- out_weight: bfloat16 [1024, 2048], P('tp'), may hold values from -0.1875 to 0.1875
- residual: bfloat16 [2048, 2048], P('sp', 'tp'), may hold values from -3 to 3
- norm_gain: float32 [2048], P('tp'), may hold values from 0.1 to 1.9
- routes: int32 [2048, 2], P('sp'), may hold values from 0 to 7, all different within a row; in each aligned block of 256 rows (0 to 255, 256 to 511, ...) at most 81 rows name the same one
- route_weights: float32 [2048, 2], P('sp'), may hold values from 0.5 to 1.5
- w_gate: bfloat16 [8, 2048, 4096], P('sp', None, 'tp'), may hold values from -0.125 to 0.125
- w_up: bfloat16 [8, 2048, 4096], P('sp', None, 'tp'), may hold values from -0.125 to 0.125
- w_down: bfloat16 [8, 4096, 2048], P('sp', 'tp'), may hold values from -0.1875 to 0.1875
Outputs:
- layer_out: bfloat16 [2048, 2048], P('sp', 'tp')
Inputs may be any that keep to these rules, and one draw needn't show every extreme that they name: `routes`: each row names 2 different experts. Among the 256 rows of one index of sp, no expert is named more than 81 times, a bound that some block reaches.
All inputs are finite; a program needn't handle non-finite values.
Results may differ from a plain program's by a relative error of at most 0.02.
The roundings to bfloat16 on the way count: a program that leaves them out, or rounds other values in their place, can miss the bound.
Values may be sent and summed in bfloat16 or wider, within the bound.
No kernel may reach another device: no remote copies, remote signals or barrier semaphores. Data moves between devices by JAX's collectives and lax.ppermute only.
A program may use at most 64 MiB of HBM per device.

v0:
```python
import jax
import jax.numpy as jnp
from jax import lax
from jax.sharding import PartitionSpec as P

D = 2048
HQ = 16
KV = 4
E = 64
TOPK = 2
GRID_W = 64


norm_eps = 1e-06
rope_base = 10000.0


def normalize(values_f, gain):
    mean_sq = jnp.mean(values_f * values_f, axis=-1, keepdims=True)
    return values_f * lax.rsqrt(mean_sq + norm_eps) * gain


def rotate(values_f, positions):
    head_width = values_f.shape[-1]
    half_width = head_width // 2
    quarter_width = half_width // 2
    frequency = rope_base ** (-jnp.arange(quarter_width, dtype=jnp.float32) / quarter_width)
    grid_rows = (positions // GRID_W).astype(jnp.float32)
    grid_cols = (positions % GRID_W).astype(jnp.float32)
    shape = (values_f.shape[0],) + (1,) * (values_f.ndim - 2) + (quarter_width,)
    pieces = []
    for coords, offset_lo in ((grid_rows, 0), (grid_cols, half_width)):
        angles = coords[:, None] * frequency[None, :]
        cosine = jnp.cos(angles).reshape(shape)
        sines = jnp.sin(angles).reshape(shape)
        first_part = values_f[..., offset_lo : offset_lo + quarter_width]
        second_part = values_f[..., offset_lo + quarter_width : offset_lo + half_width]
        pieces.append(first_part * cosine - second_part * sines)
        pieces.append(second_part * cosine + first_part * sines)
    return jnp.concatenate(pieces, axis=-1)


def shards(
    query_heads,
    key_heads,
    value_heads,
    q_gain,
    k_gain,
    out_weight,
    residual,
    norm_gain,
    routes,
    route_weights,
    w_gate,
    w_up,
    w_down,
):
    tok_rows = query_heads.shape[0]
    head_local = query_heads.shape[1] // E
    group_size = HQ // KV
    kv_count = max(head_local // group_size, 1)
    per_kv = head_local // kv_count
    tp_index = lax.axis_index("tp")
    sp_index = lax.axis_index("sp")
    kv_first = tp_index * head_local // group_size
    positions = sp_index * tok_rows + jnp.arange(tok_rows, dtype=jnp.int32)
    query_f = query_heads.astype(jnp.float32).reshape(tok_rows, kv_count, per_kv, E)
    q_turned = rotate(normalize(query_f, q_gain), positions).astype(jnp.bfloat16)
    key_cols = lax.dynamic_slice_in_dim(key_heads, kv_first * E, kv_count * E, 1)
    value_cols = lax.dynamic_slice_in_dim(value_heads, kv_first * E, kv_count * E, 1)
    key_f = key_cols.astype(jnp.float32).reshape(tok_rows, kv_count, E)
    k_turned = rotate(normalize(key_f, k_gain), positions).astype(jnp.bfloat16)
    value_sel = value_cols.reshape(tok_rows, kv_count, E)
    run_max = jnp.full((kv_count, per_kv, tok_rows), -1e30, jnp.float32)
    key_block = lax.all_gather(k_turned, "sp", axis=0, tiled=True)
    value_block = lax.all_gather(value_sel, "sp", axis=0, tiled=True)
    scores = jnp.einsum(
        "qcge,kce->cgqk", q_turned, key_block, preferred_element_type=jnp.float32
    ) * E ** (-0.5)
    new_max = jnp.maximum(run_max, jnp.max(scores, axis=-1))
    exped = jnp.exp(scores - new_max[..., None])
    denominator = jnp.sum(exped, axis=-1)
    weighted = jnp.einsum(
        "cgqk,kce->cgqe",
        exped.astype(jnp.bfloat16),
        value_block,
        preferred_element_type=jnp.float32,
    )
    run_max, denominator, weighted = (new_max, denominator, weighted)
    attended = (weighted / denominator[..., None]).astype(jnp.bfloat16)
    attended = attended.transpose(2, 0, 1, 3).reshape(tok_rows, head_local * E)
    partial_value = jnp.dot(attended, out_weight, preferred_element_type=jnp.float32).astype(
        jnp.bfloat16
    )
    attn_out = lax.psum_scatter(partial_value, "tp", scatter_dimension=1, tiled=True).astype(
        jnp.float32
    )
    after_attn = residual.astype(jnp.float32) + attn_out
    square_sum = lax.psum(jnp.sum(after_attn * after_attn, axis=1), "tp")
    normed = (after_attn * lax.rsqrt(square_sum / D + norm_eps)[:, None] * norm_gain).astype(
        jnp.bfloat16
    )
    experts_n = lax.axis_size("sp")
    capacity = 5 * tok_rows * TOPK // (4 * experts_n) + 1
    assign = routes.reshape(tok_rows * TOPK)
    onehot = (assign[:, None] == jnp.arange(experts_n, dtype=jnp.int32)[None, :]).astype(jnp.int32)
    before = jnp.cumsum(onehot, axis=0) - onehot
    slot_rank = jnp.sum(before * onehot, axis=1)
    slot_index = assign * capacity + slot_rank
    token_local = jnp.arange(tok_rows * TOPK, dtype=jnp.int32) // TOPK
    slot_token = (
        jnp.full((experts_n * capacity,), tok_rows, jnp.int32).at[slot_index].set(token_local)
    )
    gate_w = w_gate[0]
    up_w = w_up[0]
    down_w = w_down[0]
    padded = jnp.concatenate([normed, jnp.zeros((1, normed.shape[1]), jnp.bfloat16)], axis=0)
    slot_rows = padded[slot_token].reshape(experts_n, capacity, normed.shape[1])
    block_rows = lax.all_gather(
        lax.all_to_all(slot_rows, "sp", split_axis=0, concat_axis=0, tiled=True),
        "tp",
        axis=2,
        tiled=True,
    )
    gate_next = jnp.einsum("scd,df->scf", block_rows, gate_w, preferred_element_type=jnp.float32)
    up_next = jnp.einsum("scd,df->scf", block_rows, up_w, preferred_element_type=jnp.float32)
    activated = (jax.nn.silu(gate_next) * up_next).astype(jnp.bfloat16)
    partials = jnp.einsum(
        "scf,fd->scd", activated, down_w, preferred_element_type=jnp.float32
    ).astype(jnp.bfloat16)
    expert_rows = (
        lax.psum_scatter(partials, "tp", scatter_dimension=2, tiled=True)
        .astype(jnp.float32)
        .astype(jnp.bfloat16)
    )
    returned_rows = lax.all_to_all(expert_rows, "sp", split_axis=0, concat_axis=0, tiled=True)
    columns = returned_rows.shape[2]
    picked = returned_rows.reshape(experts_n * capacity, columns)[slot_index].astype(jnp.float32)
    picked = picked.reshape(tok_rows, TOPK, columns)
    expert_mix = jnp.sum(picked * route_weights[:, :, None], axis=1)
    return (after_attn + expert_mix).astype(jnp.bfloat16)


def solution(mesh):
    return jax.shard_map(
        shards,
        mesh=mesh,
        in_specs=(
            P("sp", "tp"),
            P("sp", None),
            P("sp", None),
            P(),
            P(),
            P("tp", None),
            P("sp", "tp"),
            P("tp"),
            P("sp", None),
            P("sp", None),
            P("sp", None, "tp"),
            P("sp", None, "tp"),
            P("sp", "tp", None),
        ),
        out_specs=P("sp", "tp"),
        check_vma=False,
    )
```

profile of v0, /device:TPU:0, one launch (start us, length us, event | category | flops | bytes accessed | tf_op | source)
XLA Modules:
  0.0 260.0 jit_solution(18293213865418719815)
XLA Ops:
  6.5 0.0 copy-start
  6.5 0.0 reduce-scatter.3.cloned.1.call-start
  6.6 1.0 constant_dynamic-slice_fusion.1
  7.6 0.1 copy.29
  7.7 0.7 fusion.37
  8.5 0.2 multiply_cosine_fusion.1
  8.7 0.2 fusion.55
  8.9 15.9 %all_gather.9 = bf16[2048,1,64]{0,2,1:T(8,128)(2,1)S(1)} all-gather(bf16[256,1,64]{0,2,1:T(8,128)(2,1)S(1)} %pad_maximum_fusion), channel_id=1, replica_groups=mesh['sp'=8,'tp'=4] {'sp'}, dimensions={0}, use_global_device_ids=true | all-gather | bytes 294912 | tf_op jit(solution)/shard_map/all_gather | solution.py:75
  24.8 1.0 copy.20
  25.9 0.7 multiply_multiply_fusion
  26.7 0.0 copy-start.4
  26.7 4.5 %bitcast_reduce_fusion = (f32[4,256]{1,0:T(4,128)S(1)}, f32[2048,256,4]{1,0,2:T(8,128)}) fusion(bf16[256,4,16]{0,2,1:T(8,128)(2,1)S(1)} %get-tuple-element.9, bf16[256,4,16]{0,2,1:T(8,128)(2,1)S(1)} %get-tuple-element.10, bf16[256,4,16]{0,2,1:T(8,128)(2,1)S(1)} %get-tuple-element.6, bf16[256,4,16]{0,2,1:T(8,128)(2,1)S(1)} %get-tuple-element.5, ...), kind=kOutput, calls=%fused_computation.4 | convolution fusion | flops 273153024 | bytes 8785920 | tf_op jit(solution)/shard_map/qcge,kce->cgqk/dot_general | solution.py:77
  31.2 0.0 copy-done.4
  31.2 0.1 constant_dynamic-slice_fusion
  31.3 0.1 copy.28
  31.4 14.2 %all-gather = bf16[2048,64]{0,1:T(8,128)(2,1)S(1)} all-gather(bf16[256,64]{0,1:T(8,128)(2,1)S(1)} %copy.28), channel_id=2, replica_groups=mesh['sp'=8,'tp'=4] {'sp'}, dimensions={0}, use_global_device_ids=true | all-gather | bytes 294912 | tf_op jit(solution)/shard_map/all_gather | solution.py:76
  45.6 0.0 copy-start.1
  45.6 4.9 %fusion.1 = f32[4,256]{1,0:T(4,128)S(1)} fusion(f32[2048,256,4]{1,0,2:T(8,128)} %get-tuple-element.24, f32[4,256]{1,0:T(4,128)S(1)} %broadcast_maximum_fusion), kind=kLoop, calls=%fused_computation.6 | loop fusion | flops 6290432 | bytes 8396800 | tf_op jit(solution)/shard_map/reduce_sum | solution.py:82
  50.5 0.9 copy-done.1
  51.4 1.5 fusion.20
  52.9 0.0 copy-start.2
  52.9 0.0 copy-start.6
  52.9 0.0 copy-done
  52.9 1.5 convolution_convert_fusion
  54.4 0.0 reduce-scatter.3.cloned.1.call-update
  54.4 0.0 all-gather.3.cloned.1.call-start
  54.4 0.0 copy-done.5
  54.5 0.1 copy.24
  54.6 0.1 eq.32
  54.7 0.1 eq.28
  54.9 1.1 reduce-window.6
  56.0 0.2 slice_reduce_fusion
  56.3 0.1 copy.23
  56.5 0.1 mul.365
  56.6 0.1 fusion.59
  56.7 2.4 scatter_custom_fusion
  59.2 24.4 %reduce-scatter.3.cloned.1.call-done = bf16[256,512]{1,0:T(8,128)(2,1)} async-done(((bf16[256,2048]{1,0:T(8,128)(2,1)}), bf16[256,512]{1,0:T(8,128)(2,1)}) %reduce-scatter.3.cloned.1.call-update) | async-done | bytes 262160 | tf_op jit(solution)/shard_map/reduce_scatter | solution.py:95
  83.6 0.0 copy-done.2
  83.6 1.1 multiply_reduce_fusion.1
  84.7 8.9 %psum.7 = f32[256]{0:T(256)S(1)} all-reduce(f32[256]{0:T(256)S(1)} %multiply_reduce_fusion.1), channel_id=1, replica_groups=mesh['sp'=8,'tp'=4] {'tp'}, use_global_device_ids=true, to_apply=%region_6.7 | all-reduce | flops 256 | bytes 2048 | tf_op jit(solution)/shard_map/psum | solution.py:99
  93.7 0.0 copy-done.6
  93.7 1.1 multiply_convert_fusion.1
  94.8 2.8 %gather_fusion = bf16[648,512]{1,0:T(8,128)(2,1)S(1)} fusion(bf16[257,512]{1,0:T(8,128)(2,1)S(1)} %concatenate.36, s32[1024]{0:T(1024)S(1)} %pad_clamp_fusion.1), kind=kCustom, calls=%fused_computation | custom fusion | bytes 1329696 | tf_op jit(solution)/shard_map/gather | solution.py:118
  97.6 0.2 reshape.562
  97.8 24.0 %all_to_all.10 = bf16[8,81,512]{2,1,0:T(8,128)(2,1)} all-to-all(bf16[8,81,512]{2,1,0:T(8,128)(2,1)S(1)} %reshape.562), channel_id=1, replica_groups=mesh['sp'=8,'tp'=4] {'sp'}, dimensions={0} | all-to-all | bytes 1327104 | tf_op jit(solution)/shard_map/all_to_all | solution.py:120
  121.8 0.0 all-gather.3.cloned.1.call-update
  121.9 0.2 reduce-scatter.5.cloned.1.call-start
  122.1 39.4 %all-gather.3.cloned.1.call-done = bf16[8,81,2048]{2,1,0:T(8,128)(2,1)} async-done(((bf16[8,81,512]{2,1,0:T(8,128)(2,1)}), bf16[8,81,2048]{2,1,0:T(8,128)(2,1)}) %all-gather.3.cloned.1.call-update) | async-done | bytes 2654224 | tf_op jit(solution)/shard_map/all_gather | solution.py:119
  161.5 7.8 %fusion.6 = f32[8,81,1024]{2,1,0:T(8,128)} fusion(bf16[8,81,2048]{2,1,0:T(8,128)(2,1)} %all-gather.3.cloned.1.call-done, bf16[1,2048,1024]{2,1,0:T(8,128)(2,1)} %param.24), kind=kOutput, calls=%fused_computation.11 | convolution fusion | flops 2717908992 | bytes 9502720 | tf_op jit(solution)/shard_map/scd,df->scf/dot_general | solution.py:126
  169.3 13.1 %fusion.12 = bf16[8,81,2048]{2,1,0:T(8,128)(2,1)} fusion(bf16[1,1024,2048]{2,1,0:T(8,128)(2,1)} %param.25, f32[8,81,1024]{2,1,0:T(8,128)} %fusion.6, bf16[8,81,2048]{2,1,0:T(8,128)(2,1)} %all-gather.3.cloned.1.call-done, bf16[1,2048,1024]{2,1,0:T(8,128)(2,1)} %param.23), kind=kOutput, calls=%fused_computation.16 | convolution fusion | flops 5441126400 | bytes 16351232 | tf_op jit(solution)/shard_map/scf,fd->scd/dot_general | solution.py:128
  182.4 0.0 copy-start.7
  182.4 0.0 reduce-scatter.5.cloned.1.call-update
  182.4 41.9 %reduce-scatter.5.cloned.1.call-done = bf16[8,81,512]{2,1,0:T(8,128)(2,1)} async-done(((bf16[8,81,2048]{2,1,0:T(8,128)(2,1)}), bf16[8,81,512]{2,1,0:T(8,128)(2,1)}) %reduce-scatter.5.cloned.1.call-update) | async-done | bytes 663568 | tf_op jit(solution)/shard_map/reduce_scatter | solution.py:132
  224.3 4.6 %all-to-all-start.1 = ((bf16[8,81,512]{2,1,0:T(8,128)(2,1)}), bf16[8,81,512]{2,1,0:T(8,128)(2,1)S(1)}, u32[]{:S(2)}, u32[]{:S(2)}) async-start(bf16[8,81,512]{2,1,0:T(8,128)(2,1)} %reduce-scatter.5.cloned.1.call-done), calls=%async_computation.3 | async-start | bytes 1441792 | tf_op jit(solution)/shard_map/all_to_all | solution.py:136
  228.9 0.0 copy-done.7
  228.9 0.1 copy.26
  229.0 19.4 %all-to-all-done.1 = bf16[8,81,512]{2,1,0:T(8,128)(2,1)S(1)} async-done(((bf16[8,81,512]{2,1,0:T(8,128)(2,1)}), bf16[8,81,512]{2,1,0:T(8,128)(2,1)S(1)}, u32[]{:S(2)}, u32[]{:S(2)}) %all-to-all-start.1) | async-done | bytes 663584 | tf_op jit(solution)/shard_map/all_to_all | solution.py:136
  248.4 0.2 reshape.563
  248.6 0.0 copy-start.3
  248.6 2.0 gather_fusion.1
  250.6 0.7 reshape.566
  251.3 1.3 multiply_reduce_fusion
  252.6 0.0 copy-done.3
  252.6 0.8 add_convert_fusion
  (21 shorter events, 0.3 us)
Async XLA Ops:
  6.5 46.4 %copy-start = (bf16[256,2048]{1,0:T(8,128)(2,1)S(1)}, bf16[256,2048]{1,0:T(8,128)(2,1)}, u32[]{:S(2)}) copy-start(bf16[256,2048]{1,0:T(8,128)(2,1)} %param.18) | copy-start | bytes 3145732
  6.5 77.1 %reduce-scatter.3.cloned.1.call-start = ((), (), s32[]{:S(2)}) async-start(), calls=%async_computation.4 | async-start | bytes 1310720 | tf_op jit(solution)/shard_map/reduce_scatter | solution.py:95
  26.7 4.5 %copy-start.4 = (bf16[256,256]{1,0:T(8,128)(2,1)S(1)}, bf16[256,256]{1,0:T(8,128)(2,1)}, u32[]{:S(2)}) copy-start(bf16[256,256]{1,0:T(8,128)(2,1)} %param.15) | copy-start | bytes 393220
  45.6 5.8 %copy-start.1 = (f32[2048,256,4]{1,0,2:T(8,128)S(1)}, f32[2048,256,4]{1,0,2:T(8,128)}, u32[]{:S(2)}) copy-start(f32[2048,256,4]{1,0,2:T(8,128)} %get-tuple-element.24) | copy-start | bytes 25165828
  51.4 3.1 %copy-start.5 = (s32[256,2]{0,1:T(2,128)S(1)}, s32[256,2]{0,1:T(2,128)}, u32[]{:S(2)}) copy-start(s32[256,2]{0,1:T(2,128)} %param.21) | copy-start | bytes 6148
  52.9 30.7 %copy-start.2 = (bf16[256,512]{1,0:T(8,128)(2,1)S(1)}, bf16[256,512]{1,0:T(8,128)(2,1)}, u32[]{:S(2)}) copy-start(bf16[256,512]{1,0:T(8,128)(2,1)} %param.19) | copy-start | bytes 786436
  52.9 40.8 %copy-start.6 = (f32[512]{0:T(512)S(1)}, f32[512]{0:T(512)}, u32[]{:S(2)}) copy-start(f32[512]{0:T(512)} %param.20) | copy-start | bytes 6148
  54.4 107.1 %all-gather.3.cloned.1.call-start = ((), (), s32[]{:S(2)}) async-start(), calls=%async_computation.5 | async-start | bytes 3604480 | tf_op jit(solution)/shard_map/all_gather | solution.py:119
  121.9 102.4 %reduce-scatter.5.cloned.1.call-start = ((), (), s32[]{:S(2)}) async-start(), calls=%async_computation.6 | async-start | bytes 3604480 | tf_op jit(solution)/shard_map/reduce_scatter | solution.py:132
  182.4 46.5 %copy-start.7 = (f32[256,2]{0,1:T(2,128)S(1)}, f32[256,2]{0,1:T(2,128)}, u32[]{:S(2)}) copy-start(f32[256,2]{0,1:T(2,128)} %param.22) | copy-start | bytes 6148
  224.3 24.1 %all-to-all-start.1 = ((bf16[8,81,512]{2,1,0:T(8,128)(2,1)}), bf16[8,81,512]{2,1,0:T(8,128)(2,1)S(1)}, u32[]{:S(2)}, u32[]{:S(2)}) async-start(bf16[8,81,512]{2,1,0:T(8,128)(2,1)} %reduce-scatter.5.cloned.1.call-done), calls=%async_computation.3 | async-start | bytes 1441792 | tf_op jit(solution)/shard_map/all_to_all | solution.py:136
  248.6 4.0 %copy-start.3 = (bf16[256,512]{1,0:T(8,128)(2,1)S(1)}, bf16[256,512]{1,0:T(8,128)(2,1)}, u32[]{:S(2)}) copy-start(bf16[256,512]{1,0:T(8,128)(2,1)} %reduce-scatter.3.cloned.1.call-done) | copy-start | bytes 786436
Sparse Core Ops, SparseCore 0:
  54.5 29.0 reduce-scatter.2
  122.0 39.4 all-gather.2
  182.5 41.6 reduce-scatter.4
where the time goes:
time: 260 us
  waiting for transfers between devices  125 us (48%)
  blocking collectives  63.1 us (24%)
  matrix products  28.3 us (11%)
  between operations  13.4 us (5%)
  other arithmetic  12.6 us (5%)
  local copies, waits for them, and re-layouts  12.5 us (5%)
  starting transfers between devices  4.87 us (2%)
    reduce_scatter x1, waiting for transfers between devices, shards(): lax.psum_scatter(partials, 'tp', scatter_dimension=2, tiled=True)  41.9 us
    all_gather x1, waiting for transfers between devices, shards(): lax.all_gather(lax.all_to_all(slot_rows, 'sp', split_axis=0, concat_axis=...  39.4 us
    reduce_scatter x1, waiting for transfers between devices, shards(): lax.psum_scatter(partial_value, 'tp', scatter_dimension=1, tiled=True)  24.4 us
    all_to_all x1, blocking collectives, shards(): lax.all_to_all(slot_rows, 'sp', split_axis=0, concat_axis=0, tiled=True)  24 us
    all_to_all x1, waiting for transfers between devices, shards(): lax.all_to_all(expert_rows, 'sp', split_axis=0, concat_axis=0, tiled=True)  19.4 us
    all_gather x1, blocking collectives, shards(): key_block = lax.all_gather(k_turned, 'sp', axis=0, tiled=True)  15.9 us
    all_gather x1, blocking collectives, shards(): value_block = lax.all_gather(value_sel, 'sp', axis=0, tiled=True)  14.2 us
    dot_general x1, matrix products, shards(): jnp.einsum('scf,fd->scd', activated, down_w, preferred_element_type=jnp.f...  13.1 us
  transfers between devices with their start and end apart: 4, of which 4 were waited for; matrix products, arithmetic and copies ran while one was open for 2% of the time, Pallas kernels for 0%

commit v1 on v0

v1 whole, which is shorter than its diff:
```python
import jax
import jax.numpy as jnp
from jax import lax
from jax.experimental import pallas as pl
from jax.experimental.pallas import tpu as pltpu
from jax.sharding import PartitionSpec as P

D = 2048
HQ = 16
KV = 4
E = 64
TOPK = 2
GRID_W = 64
GROUPS = 4

norm_eps = 1e-06
rope_base = 10000.0
bf16 = jnp.bfloat16
f32 = jnp.float32


def turn(values, gain, heads, positions):
    rows, width = values.shape
    lane = jnp.arange(width, dtype=jnp.int32) % E
    quarter = E // 4
    same_head = (jnp.arange(width)[:, None] // E == jnp.arange(heads)[None, :]).astype(f32)
    mean_sq = jnp.dot(values * values, same_head, precision=lax.Precision.HIGHEST) / E
    scale = jnp.dot(
        lax.rsqrt(mean_sq + norm_eps), same_head.T, precision=lax.Precision.HIGHEST
    )
    normed = values * scale * jnp.tile(gain, heads)[None, :]
    frequency = rope_base ** (-jnp.arange(quarter, dtype=f32) / quarter)
    grid_rows = (positions // GRID_W).astype(f32)
    grid_cols = (positions % GRID_W).astype(f32)
    angles = jnp.concatenate(
        [grid_rows[:, None] * frequency[None, :], grid_cols[:, None] * frequency[None, :]], axis=1
    )
    cosine = jnp.cos(angles)
    sines = jnp.sin(angles)
    cos_lane = jnp.concatenate([cosine[:, :quarter]] * 2 + [cosine[:, quarter:]] * 2, axis=1)
    sin_lane = jnp.concatenate(
        [-sines[:, :quarter], sines[:, :quarter], -sines[:, quarter:], sines[:, quarter:]], axis=1
    )
    first = (lane % (2 * quarter)) < quarter
    other = jnp.where(
        first[None, :], jnp.roll(normed, -quarter, axis=1), jnp.roll(normed, quarter, axis=1)
    )
    return (
        normed * jnp.tile(cos_lane, (1, heads)) + other * jnp.tile(sin_lane, (1, heads))
    ).astype(bf16)


def write_parts(value, offs_ref, outs, blocks, width):
    for ref, indices in zip(outs, blocks):
        for place, index in enumerate(indices):
            start = offs_ref[index]
            if width < D:
                start = pl.multiple_of(start, 128)
                ref[:, place * width : (place + 1) * width] = value[:, pl.ds(start, width)].astype(
                    bf16
                )
            else:
                ref[...] = value[...].astype(bf16)


def attention_kernel(blocks, width, kv_count, per_kv, pieces):
    def body(offs_ref, q_ref, *refs):
        kv_refs = refs[:pieces]
        weight_ref = refs[pieces]
        outs = refs[pieces + 1 : pieces + 1 + len(blocks)]
        kv_all, attended, acc = refs[pieces + 1 + len(blocks) :]
        rows = kv_refs[0].shape[0]
        for n in range(pieces):
            kv_all[n * rows : (n + 1) * rows, :] = kv_refs[n][...]
        for c in range(kv_count):
            kv = kv_all[:, c * 2 * E : (c + 1) * 2 * E]
            for g in range(per_kv):
                h = c * per_kv + g
                q = q_ref[:, h * 2 * E : (h + 1) * 2 * E]
                scores = lax.dot_general(
                    q, kv, (((1,), (1,)), ((), ())), preferred_element_type=f32
                )
                scores = scores * (E**-0.5)
                exped = jnp.exp(scores - jnp.max(scores, axis=1, keepdims=True))
                total = jnp.sum(exped, axis=1, keepdims=True)
                mixed = jnp.dot(exped.astype(bf16), kv, preferred_element_type=f32)
                attended[:, h * E : (h + 1) * E] = (mixed[:, E:] / total).astype(bf16)
        acc[...] = jnp.dot(attended[...], weight_ref[...], preferred_element_type=f32)
        write_parts(acc, offs_ref, outs, blocks, width)

    return body


def expert_kernel(blocks, width, in_offs, pieces, steps):
    def body(offs_ref, gain_ref, *refs):
        u_refs = refs[:pieces]
        gate_ref, up_ref, down_ref = refs[pieces : pieces + 3]
        outs = refs[pieces + 3 : pieces + 3 + len(blocks)]
        acc, scale = refs[pieces + 3 + len(blocks) :]
        step = pl.program_id(0)

        @pl.when(step == 0)
        def _():
            total = None
            for n in range(pieces):
                wide = u_refs[n].shape[1]
                start = pl.multiple_of(offs_ref[in_offs[n]], 128)
                plain = u_refs[n][...].astype(f32) / gain_ref[:, pl.ds(start, wide)]
                part = jnp.sum(plain * plain, axis=1, keepdims=True)
                total = part if total is None else total + part
            scale[...] = jnp.broadcast_to(lax.rsqrt(total / D + norm_eps), scale.shape)

        gate = None
        up = None
        for n in range(pieces):
            wide = u_refs[n].shape[1]
            start = pl.multiple_of(offs_ref[in_offs[n]], 128)
            u = u_refs[n][...]
            g = jnp.dot(u, gate_ref[0, pl.ds(start, wide), :], preferred_element_type=f32)
            v = jnp.dot(u, up_ref[0, pl.ds(start, wide), :], preferred_element_type=f32)
            gate = g if gate is None else gate + g
            up = v if up is None else up + v
        factor = scale[:, 0:1]
        gate = gate * factor
        up = up * factor
        act = (gate / (1.0 + jnp.exp(-gate)) * up).astype(bf16)
        part = jnp.dot(act, down_ref[0], preferred_element_type=f32)

        @pl.when(step == 0)
        def _():
            acc[...] = part

        @pl.when(step > 0)
        def _():
            acc[...] += part

        @pl.when(step == steps - 1)
        def _():
            write_parts(acc, offs_ref, outs, blocks, width)

    return body


def shards(
    query_heads,
    key_heads,
    value_heads,
    q_gain,
    k_gain,
    out_weight,
    residual,
    norm_gain,
    routes,
    route_weights,
    w_gate,
    w_up,
    w_down,
):
    tok_rows = query_heads.shape[0]
    head_local = query_heads.shape[1] // E
    group_size = HQ // KV
    kv_count = max(head_local // group_size, 1)
    per_kv = head_local // kv_count
    tp_index = lax.axis_index("tp")
    sp_index = lax.axis_index("sp")
    sp_n = lax.axis_size("sp")
    tp_n = lax.axis_size("tp")
    columns = residual.shape[1]
    square = tp_n == 4
    half = columns // 2

    def sp_swap(x, s):
        return lax.ppermute(x, "sp", [(i, i ^ s) for i in range(sp_n)])

    def tp_swap(x, s):
        return lax.ppermute(x, "tp", [(i, i ^ s) for i in range(tp_n)])

    if square:
        offs = jnp.stack(
            [(tp_index ^ s) * columns + h * half for s in range(4) for h in range(2)]
        ).astype(jnp.int32)
        blocks = [(2, 6), (5, 7), (0, 4), (1, 3)]
        width = half
    else:
        offs = jnp.zeros((1,), jnp.int32)
        blocks = [(0,)]
        width = D

    def scatter_sum(parts):
        if not square:
            return lax.psum_scatter(parts[0], "tp", scatter_dimension=1, tiled=True).astype(f32)
        far_a, far_b, near_a, near_b = parts
        sum_a = near_a.astype(f32) + tp_swap(far_a, 1).astype(f32)
        sum_b = near_b.astype(f32) + tp_swap(far_b, 2).astype(f32)
        last_a = tp_swap(sum_a[:, half:].astype(bf16), 2)
        last_b = tp_swap(sum_b[:, half:].astype(bf16), 1)
        return jnp.concatenate(
            [sum_a[:, :half] + last_a.astype(f32), sum_b[:, :half] + last_b.astype(f32)], axis=1
        )

    kv_first = tp_index * head_local // group_size
    positions = sp_index * tok_rows + jnp.arange(tok_rows, dtype=jnp.int32)
    key_cols = lax.dynamic_slice_in_dim(key_heads, kv_first * E, kv_count * E, 1)
    value_cols = lax.dynamic_slice_in_dim(value_heads, kv_first * E, kv_count * E, 1)
    k_turned = turn(key_cols.astype(f32), k_gain, kv_count, positions)
    kv_own = jnp.concatenate(
        [
            part[:, c * E : (c + 1) * E]
            for c in range(kv_count)
            for part in (k_turned, value_cols)
        ],
        axis=1,
    )
    firsts = [kv_own] + [sp_swap(kv_own, s) for s in range(2, sp_n, 2)]
    firsts = jnp.concatenate(firsts, axis=0)
    kv_pieces = [firsts, sp_swap(firsts, 1)]
    q_turned = turn(query_heads.astype(f32), q_gain, head_local, positions)
    q_wide = jnp.concatenate(
        [q_turned.reshape(tok_rows, head_local, E), jnp.zeros((tok_rows, head_local, E), bf16)],
        axis=2,
    ).reshape(tok_rows, head_local * 2 * E)

    capacity = 5 * tok_rows * TOPK // (4 * sp_n) + 1
    slots = -(-capacity // 8) * 8
    order = sp_index ^ jnp.arange(sp_n, dtype=jnp.int32)
    named = (routes[:, :, None] == order[None, None, :]).astype(f32)
    counts = jnp.sum(named, axis=1)
    below = (
        jnp.arange(tok_rows)[:, None] > jnp.arange(tok_rows)[None, :]
    ).astype(bf16)
    before = jnp.dot(below, counts.astype(bf16), preferred_element_type=f32)
    slot_at = jnp.where(counts > 0, before, -1.0)
    pick = (
        slot_at.T[:, None, :] == jnp.arange(slots, dtype=f32)[None, :, None]
    ).astype(bf16).reshape(sp_n * slots, tok_rows)
    slot_of_k = jnp.sum(
        named * (before + jnp.arange(sp_n, dtype=f32)[None, :] * slots)[:, None, :], axis=2
    )
    take = [
        (slot_of_k[:, k : k + 1] == jnp.arange(sp_n * slots, dtype=f32)[None, :]).astype(bf16)
        for k in range(TOPK)
    ]

    if square:
        gain_parts = [norm_gain] + [tp_swap(norm_gain, s) for s in (1, 2, 3)]
        gain_all = jnp.zeros((D,), f32)
        for s in range(4):
            gain_all = lax.dynamic_update_slice(
                gain_all, gain_parts[s], ((tp_index ^ s) * columns,)
            )
    else:
        gain_all = lax.all_gather(norm_gain, "tp", axis=0, tiled=True)
    gain_all = gain_all[None, :]

    vmem = pl.BlockSpec(memory_space=pltpu.VMEM)
    smem = pl.BlockSpec(memory_space=pltpu.SMEM)
    part_shapes = lambda rows: [
        jax.ShapeDtypeStruct((rows, width * len(indices)), bf16) for indices in blocks
    ]
    parts = pl.pallas_call(
        attention_kernel(blocks, width, kv_count, per_kv, len(kv_pieces)),
        out_shape=part_shapes(tok_rows),
        in_specs=[smem] + [vmem] * (2 + len(kv_pieces)),
        out_specs=[vmem] * len(blocks),
        scratch_shapes=[
            pltpu.VMEM((sp_n * tok_rows, kv_count * 2 * E), bf16),
            pltpu.VMEM((tok_rows, head_local * E), bf16),
            pltpu.VMEM((tok_rows, D), f32),
        ],
        compiler_params=pltpu.CompilerParams(vmem_limit_bytes=56 * 1024 * 1024),
        name="attention",
    )(offs, q_wide, *kv_pieces, out_weight)
    after_attn = residual.astype(f32) + scatter_sum(parts)
    scaled = (after_attn * norm_gain[None, :]).astype(bf16)

    sent = jnp.dot(pick, scaled, preferred_element_type=f32).astype(bf16)
    per_group = sp_n // GROUPS
    hidden = w_gate.shape[2]
    hidden_block = min(hidden, 256)
    steps = hidden // hidden_block
    picked = [None] * TOPK
    for group in range(GROUPS):
        arrived = []
        for s in range(group * per_group, (group + 1) * per_group):
            piece = sent[s * slots : (s + 1) * slots]
            arrived.append(sp_swap(piece, s) if s else piece)
        own = jnp.concatenate(arrived, axis=0)
        rows = own.shape[0]
        if square:
            side_x = tp_swap(own, 1)
            side_y = tp_swap(own, 2)
            inputs = [own, side_x, side_y, tp_swap(side_y[:, :half], 1), tp_swap(side_x[:, half:], 2)]
            in_offs = (0, 2, 4, 6, 7)
        else:
            inputs = [lax.all_gather(own, "tp", axis=1, tiled=True)]
            in_offs = (0,)
        whole = lambda x: pl.BlockSpec(x.shape, lambda f: (0, 0))
        parts = pl.pallas_call(
            expert_kernel(blocks, width, in_offs, len(inputs), steps),
            grid=(steps,),
            out_shape=part_shapes(rows),
            in_specs=[smem, whole(gain_all)]
            + [whole(x) for x in inputs]
            + [
                pl.BlockSpec((1, D, hidden_block), lambda f: (0, 0, f)),
                pl.BlockSpec((1, D, hidden_block), lambda f: (0, 0, f)),
                pl.BlockSpec((1, hidden_block, D), lambda f: (0, f, 0)),
            ],
            out_specs=[
                pl.BlockSpec((rows, width * len(indices)), lambda f: (0, 0)) for indices in blocks
            ],
            scratch_shapes=[pltpu.VMEM((rows, D), f32), pltpu.VMEM((rows, 128), f32)],
            compiler_params=pltpu.CompilerParams(vmem_limit_bytes=40 * 1024 * 1024),
            name="experts",
        )(offs, gain_all, *inputs, w_gate, w_up, w_down)
        expert_rows = scatter_sum(parts).astype(bf16)
        returned = []
        for n in range(per_group):
            s = group * per_group + n
            piece = expert_rows[n * slots : (n + 1) * slots]
            returned.append(sp_swap(piece, s) if s else piece)
        returned = jnp.concatenate(returned, axis=0)
        for k in range(TOPK):
            part = jnp.dot(
                take[k][:, group * per_group * slots : (group + 1) * per_group * slots],
                returned,
                preferred_element_type=f32,
            )
            picked[k] = part if picked[k] is None else picked[k] + part
    expert_mix = picked[0] * route_weights[:, 0:1]
    for k in range(1, TOPK):
        expert_mix = expert_mix + picked[k] * route_weights[:, k : k + 1]
    return (after_attn + expert_mix).astype(bf16)


def solution(mesh):
    return jax.shard_map(
        shards,
        mesh=mesh,
        in_specs=(
            P("sp", "tp"),
            P("sp", None),
            P("sp", None),
            P(),
            P(),
            P("tp", None),
            P("sp", "tp"),
            P("tp"),
            P("sp", None),
            P("sp", None),
            P("sp", None, "tp"),
            P("sp", None, "tp"),
            P("sp", "tp", None),
        ),
        out_specs=P("sp", "tp"),
        check_vma=False,
    )
```

time: 260 us -> 156 us (0.60)
  waiting for transfers between devices: 125 us -> 36.3 us
  starting transfers between devices: 4.87 us -> 69.9 us
  blocking collectives: 63.1 us -> 0 us
  Pallas kernels: 0 us -> 29.8 us
  matrix products: 28.3 us -> 5.37 us
  between operations: 13.4 us -> 1.04 us
  other arithmetic: 12.6 us -> 6.34 us
  local copies, waits for them, and re-layouts: 12.5 us -> 6.46 us
    ppermute x0 -> x57, starting transfers between devices: none -> 69.9 us  [the longest x39 44.2 us: tp_swap(): return lax.ppermute(x, 'tp', [(i, i ^ s) for i in range(tp_n)])]
    reduce_scatter x2 -> x0, waiting for transfers between devices: 66.3 us -> none  [the longest x1 41.9 us: shards(): lax.psum_scatter(partials, 'tp', scatter_dimension=2, tiled=True)]
    all_gather x1 -> x0, waiting for transfers between devices: 39.4 us -> none  [shards(): lax.all_gather(lax.all_to_all(slot_rows, 'sp', split_axis=0, concat_axis=...]
    ppermute x0 -> x57, waiting for transfers between devices: none -> 36.3 us  [the longest x39 18.5 us: tp_swap(): return lax.ppermute(x, 'tp', [(i, i ^ s) for i in range(tp_n)])]
    all_gather x2 -> x0, blocking collectives: 30.1 us -> none  [the longest x1 15.9 us: shards(): key_block = lax.all_gather(k_turned, 'sp', axis=0, tiled=True)]
    pallas_call x0 -> x5, Pallas kernels: none -> 29.8 us  [the longest x4 23.2 us: shards(): pl.pallas_call(expert_kernel(blocks, width, in_offs, len(inputs), steps),...]
    all_to_all x1 -> x0, blocking collectives: 24 us -> none  [shards(): lax.all_to_all(slot_rows, 'sp', split_axis=0, concat_axis=0, tiled=True)]
    dot_general x5 -> x13, matrix products: 28.3 us -> 5.37 us  [the longest x8 3.02 us: shards(): jnp.dot(take[k][:, group * per_group * slots:(group + 1) * per_group * sl...]
  transfers between devices with their start and end apart: 4 -> 57, of which waited for: 4 -> 17; matrix products, arithmetic and copies ran while one was open for 2% -> 6% of each run, Pallas kernels for 0% -> 19%
where the time goes in v1:
time: 156 us; the launch traced here: 155 us
  starting transfers between devices  69.9 us (45%)
  waiting for transfers between devices  36.3 us (23%)
  Pallas kernels  29.8 us (19%)
  local copies, waits for them, and re-layouts  6.46 us (4%)
  other arithmetic  6.34 us (4%)
  matrix products  5.37 us (3%)
    ppermute x39, starting transfers between devices, tp_swap(): return lax.ppermute(x, 'tp', [(i, i ^ s) for i in range(tp_n)])  44.2 us
    ppermute x18, starting transfers between devices, sp_swap(): return lax.ppermute(x, 'sp', [(i, i ^ s) for i in range(sp_n)])  25.7 us
    pallas_call x4, Pallas kernels, shards(): pl.pallas_call(expert_kernel(blocks, width, in_offs, len(inputs), steps),...  23.2 us
    ppermute x39, waiting for transfers between devices, tp_swap(): return lax.ppermute(x, 'tp', [(i, i ^ s) for i in range(tp_n)])  18.5 us
    ppermute x18, waiting for transfers between devices, sp_swap(): return lax.ppermute(x, 'sp', [(i, i ^ s) for i in range(sp_n)])  17.8 us
    pallas_call x1, Pallas kernels, shards(): pl.pallas_call(attention_kernel(blocks, width, kv_count, per_kv, len(kv_p...  6.52 us
    unnamed x38, local copies, waits for them, and re-layouts  3.8 us
  transfers between devices with their start and end apart: 57, of which 17 were waited for; matrix products, arithmetic and copies ran while one was open for 6% of the time, Pallas kernels for 19%

profile of v1, /device:TPU:0, one launch (start us, length us, event | category | flops | bytes accessed | tf_op | source)
XLA Modules:
  0.0 155.2 jit_solution(9127326611398871802)
XLA Ops:
  0.1 1.1 fusion.39
  1.2 1.0 fusion.40
  3.5 1.2 fusion.43
  4.8 3.1 %collective-permute-start = (bf16[256,128]{1,0:T(8,128)(2,1)S(1)}, bf16[256,128]{1,0:T(8,128)(2,1)S(1)}, u32[]{:S(2)}, u32[]{:S(2)}) collective-permute-start(bf16[256,128]{1,0:T(8,128)(2,1)S(1)} %pad_maximum_fusion.11), channel_id=1, source_target_pairs={{0,8},{4,12},{8,0},{12,4},{16,24},{20,28},{24,16},{28,20},{1,9},{5... | collective-permute-start | bytes 196616 | tf_op jit(solution)/shard_map/ppermute | solution.py:173
  7.9 2.6 %collective-permute-start.1 = (bf16[256,128]{1,0:T(8,128)(2,1)S(1)}, bf16[256,128]{1,0:T(8,128)(2,1)S(1)}, u32[]{:S(2)}, u32[]{:S(2)}) collective-permute-start(bf16[256,128]{1,0:T(8,128)(2,1)S(1)} %pad_maximum_fusion.11), channel_id=1, source_target_pairs={{0,16},{4,20},{8,24},{12,28},{16,0},{20,4},{24,8},{28,12},{1,17},{... | collective-permute-start | bytes 196616 | tf_op jit(solution)/shard_map/ppermute | solution.py:173
  10.5 1.7 %collective-permute-start.8 = (f32[512]{0:T(512)S(1)}, f32[512]{0:T(512)S(1)}, u32[]{:S(2)}, u32[]{:S(2)}) collective-permute-start(f32[512]{0:T(512)S(1)} %copy-done.11), channel_id=1, source_target_pairs={{0,1},{1,0},{2,3},{3,2},{4,5},{5,4},{6,7},{7,6},{8,9},{9,8},{10,11... | collective-permute-start | bytes 6152 | tf_op jit(solution)/shard_map/ppermute | solution.py:176
  12.2 1.5 collective-permute-start.9
  15.2 1.4 collective-permute-done.2
  19.5 6.5 %attention.1 = (bf16[256,512]{1,0:T(8,128)(2,1)}, bf16[256,512]{1,0:T(8,128)(2,1)}, bf16[256,512]{1,0:T(8,128)(2,1)}, bf16[256,512]{1,0:T(8,128)(2,1)}) custom-call(s32[8]{0:T(128)} %stack.35.offs_ref, bf16[256,512]{1,0:T(8,128)(2,1)} %bitcast.44, bf16[1024,128]{1,0:T(8,128)(2,1)} %copy-done.8, bf16[1024,128]{1,0:T(8,128)(2,1)} %copy-done.9, ...), custom_call_target="tpu_custom_call" | custom-call | tf_op jit(solution)/shard_map/attention/pallas_call | solution.py:260
  26.1 1.5 collective-permute-start.4
  27.8 1.6 %collective-permute-start.6 = (bf16[256,512]{1,0:T(8,128)(2,1)}, bf16[256,512]{1,0:T(8,128)(2,1)S(1)}, u32[]{:S(2)}, u32[]{:S(2)}) collective-permute-start(bf16[256,512]{1,0:T(8,128)(2,1)} %get-tuple-element.28), channel_id=1, source_target_pairs={{0,2},{1,3},{2,0},{3,1},{4,6},{5,7},{6,4},{7,5},{8,10},{9,11},{10,... | collective-permute-start | bytes 786440 | tf_op jit(solution)/shard_map/ppermute | solution.py:176
  29.8 5.2 %collective-permute-done.4 = bf16[256,512]{1,0:T(8,128)(2,1)S(1)} collective-permute-done((bf16[256,512]{1,0:T(8,128)(2,1)}, bf16[256,512]{1,0:T(8,128)(2,1)S(1)}, u32[]{:S(2)}, u32[]{:S(2)}) %collective-permute-start.4) | collective-permute-done | bytes 262176 | tf_op jit(solution)/shard_map/ppermute | solution.py:176
  35.0 1.0 convert_add_fusion.1
  36.0 1.6 %collective-permute-start.5 = (bf16[256,256]{1,0:T(8,128)(2,1)S(1)}, bf16[256,256]{1,0:T(8,128)(2,1)S(1)}, u32[]{:S(2)}, u32[]{:S(2)}) collective-permute-start(bf16[256,256]{1,0:T(8,128)(2,1)S(1)} %slice.444), channel_id=1, source_target_pairs={{0,2},{1,3},{2,0},{3,1},{4,6},{5,7},{6,4},{7,5},{8,10},{9,11},{10,... | collective-permute-start | bytes 393224 | tf_op jit(solution)/shard_map/ppermute | solution.py:176
  37.6 1.2 convert_add_fusion
  38.8 1.6 %collective-permute-start.7 = (bf16[256,256]{1,0:T(8,128)(2,1)S(1)}, bf16[256,256]{1,0:T(8,128)(2,1)S(1)}, u32[]{:S(2)}, u32[]{:S(2)}) collective-permute-start(bf16[256,256]{1,0:T(8,128)(2,1)S(1)} %slice.443), channel_id=1, source_target_pairs={{0,1},{1,0},{2,3},{3,2},{4,5},{5,4},{6,7},{7,6},{8,9},{9,8},{10,11... | collective-permute-start | bytes 393224 | tf_op jit(solution)/shard_map/ppermute | solution.py:176
  41.2 2.7 %collective-permute-done.7 = bf16[256,256]{1,0:T(8,128)(2,1)S(1)} collective-permute-done((bf16[256,256]{1,0:T(8,128)(2,1)S(1)}, bf16[256,256]{1,0:T(8,128)(2,1)S(1)}, u32[]{:S(2)}, u32[]{:S(2)}) %collective-permute-start.7) | collective-permute-done | bytes 131104 | tf_op jit(solution)/shard_map/ppermute | solution.py:176
  44.6 1.8 %collective-permute-start.22 = (bf16[88,512]{1,0:T(8,128)(2,1)S(1)}, bf16[88,512]{1,0:T(8,128)(2,1)S(1)}, u32[]{:S(2)}, u32[]{:S(2)}) collective-permute-start(bf16[88,512]{1,0:T(8,128)(2,1)S(1)} %get-tuple-element.53), channel_id=1, source_target_pairs={{0,12},{4,8},{8,4},{12,0},{16,28},{20,24},{24,20},{28,16},{1,13},{... | collective-permute-start | bytes 270344 | tf_op jit(solution)/shard_map/ppermute | solution.py:173
  46.4 1.6 %collective-permute-start.33 = (bf16[88,512]{1,0:T(8,128)(2,1)S(1)}, bf16[88,512]{1,0:T(8,128)(2,1)S(1)}, u32[]{:S(2)}, u32[]{:S(2)}) collective-permute-start(bf16[88,512]{1,0:T(8,128)(2,1)S(1)} %get-tuple-element.52), channel_id=1, source_target_pairs={{0,16},{4,20},{8,24},{12,28},{16,0},{20,4},{24,8},{28,12},{1,17},{... | collective-permute-start | bytes 270344 | tf_op jit(solution)/shard_map/ppermute | solution.py:173
  48.0 2.1 %collective-permute-done.21 = bf16[88,512]{1,0:T(8,128)(2,1)S(1)} collective-permute-done((bf16[88,512]{1,0:T(8,128)(2,1)S(1)}, bf16[88,512]{1,0:T(8,128)(2,1)S(1)}, u32[]{:S(2)}, u32[]{:S(2)}) %collective-permute-start.21) | collective-permute-done | bytes 90144 | tf_op jit(solution)/shard_map/ppermute | solution.py:173
  50.4 1.9 %collective-permute-done.33 = bf16[88,512]{1,0:T(8,128)(2,1)S(1)} collective-permute-done((bf16[88,512]{1,0:T(8,128)(2,1)S(1)}, bf16[88,512]{1,0:T(8,128)(2,1)S(1)}, u32[]{:S(2)}, u32[]{:S(2)}) %collective-permute-start.33) | collective-permute-done | bytes 90144 | tf_op jit(solution)/shard_map/ppermute | solution.py:173
  52.3 5.7 %collective-permute-start.45 = (bf16[88,512]{1,0:T(8,128)(2,1)S(1)}, bf16[88,512]{1,0:T(8,128)(2,1)S(1)}, u32[]{:S(2)}, u32[]{:S(2)}) collective-permute-start(bf16[88,512]{1,0:T(8,128)(2,1)S(1)} %get-tuple-element.50), channel_id=1, source_target_pairs={{0,24},{4,28},{8,16},{12,20},{16,8},{20,12},{24,0},{28,4},{1,25},{... | collective-permute-start | bytes 270344 | tf_op jit(solution)/shard_map/ppermute | solution.py:173
  58.0 2.6 %collective-permute-done.45 = bf16[88,512]{1,0:T(8,128)(2,1)S(1)} collective-permute-done((bf16[88,512]{1,0:T(8,128)(2,1)S(1)}, bf16[88,512]{1,0:T(8,128)(2,1)S(1)}, u32[]{:S(2)}, u32[]{:S(2)}) %collective-permute-start.45) | collective-permute-done | bytes 90144 | tf_op jit(solution)/shard_map/ppermute | solution.py:173
  60.6 2.1 %collective-permute-start.13 = (bf16[176,512]{1,0:T(8,128)(2,1)S(1)}, bf16[176,512]{1,0:T(8,128)(2,1)S(1)}, u32[]{:S(2)}, u32[]{:S(2)}) collective-permute-start(bf16[176,512]{1,0:T(8,128)(2,1)S(1)} %pad_maximum_fusion.1.refs_0_), channel_id=1, source_target_pairs={{0,2},{1,3},{2,0},{3,1},{4,6},{5,7},{6,4},{7,5},{8,10},{9,11},{10,... | collective-permute-start | bytes 540680 | tf_op jit(solution)/shard_map/ppermute | solution.py:176
  62.9 1.5 collective-permute-start.24
  64.3 2.6 %collective-permute-done.46 = bf16[88,512]{1,0:T(8,128)(2,1)S(1)} collective-permute-done((bf16[88,512]{1,0:T(8,128)(2,1)S(1)}, bf16[88,512]{1,0:T(8,128)(2,1)S(1)}, u32[]{:S(2)}, u32[]{:S(2)}) %collective-permute-start.46) | collective-permute-done | bytes 90144 | tf_op jit(solution)/shard_map/ppermute | solution.py:173
  66.9 1.5 collective-permute-start.23
  69.0 2.0 %collective-permute-start.35 = (bf16[176,512]{1,0:T(8,128)(2,1)S(1)}, bf16[176,512]{1,0:T(8,128)(2,1)S(1)}, u32[]{:S(2)}, u32[]{:S(2)}) collective-permute-start(bf16[176,512]{1,0:T(8,128)(2,1)S(1)} %constant_dynamic-update-slice_fusion.4.refs_0_), channel_id=1, source_target_pairs={{0,1},{1,0},{2,3},{3,2},{4,5},{5,4},{6,7},{7,6},{8,9},{9,8},{10,11... | collective-permute-start | bytes 540680 | tf_op jit(solution)/shard_map/ppermute | solution.py:176
  71.1 1.4 collective-permute-start.10
  72.6 1.8 %collective-permute-done.23.refs_1_ = bf16[176,512]{1,0:T(8,128)(2,1)S(1)} collective-permute-done((bf16[176,512]{1,0:T(8,128)(2,1)S(1)}, bf16[176,512]{1,0:T(8,128)(2,1)S(1)}, u32[]{:S(2)}, u32[]{:S(2)}) %collective-permute-start.23) | collective-permute-done | bytes 180256 | tf_op jit(solution)/shard_map/ppermute | solution.py:176
  75.3 3.8 %collective-permute-done.10 = f32[512]{0:T(512)S(1)} collective-permute-done((f32[512]{0:T(512)S(1)}, f32[512]{0:T(512)S(1)}, u32[]{:S(2)}, u32[]{:S(2)}) %collective-permute-start.10) | collective-permute-done | bytes 2080 | tf_op jit(solution)/shard_map/ppermute | solution.py:176
  79.6 1.0 collective-permute-start.15
  80.6 1.1 collective-permute-start.25
  81.8 1.4 collective-permute-start.26
  84.6 1.1 collective-permute-start.38
  86.6 2.2 %copy-done.4 = bf16[1,1024,2048]{2,1,0:T(8,128)(2,1)S(1)} copy-done((bf16[1,1024,2048]{2,1,0:T(8,128)(2,1)S(1)}, bf16[1,1024,2048]{2,1,0:T(8,128)(2,1)}, u32[]{:S(2)}) %copy-start.4) | copy-done | bytes 4194328
  88.8 5.8 %experts.4 = (bf16[176,512]{1,0:T(8,128)(2,1)S(1)}, bf16[176,512]{1,0:T(8,128)(2,1)S(1)}, bf16[176,512]{1,0:T(8,128)(2,1)S(1)}, bf16[176,512]{1,0:T(8,128)(2,1)S(1)}) custom-call(s32[8]{0:T(128)S(1)} %copy-done.6, f32[1,2048]{1,0:T(1,128)S(1)} %constant_dynamic-update-slice_fusion.12.gain_ref, bf16[176,512]{1,0:T(8,128)(2,1)S(1)} %pad_maximum_fusion.1.refs_0_, ...), custom_call_target="tpu_custom_call" | custom-call | tf_op jit(solution)/shard_map/experts/pallas_call | solution.py:298
  94.6 1.0 collective-permute-start.50
  95.5 1.1 collective-permute-start.18
  96.7 5.8 %experts.5 = (bf16[176,512]{1,0:T(8,128)(2,1)S(1)}, bf16[176,512]{1,0:T(8,128)(2,1)S(1)}, bf16[176,512]{1,0:T(8,128)(2,1)S(1)}, bf16[176,512]{1,0:T(8,128)(2,1)S(1)}) custom-call(s32[8]{0:T(128)S(1)} %copy-done.6, f32[1,2048]{1,0:T(1,128)S(1)} %constant_dynamic-update-slice_fusion.12.gain_ref, ...), custom_call_target="tpu_custom_call" | custom-call | tf_op jit(solution)/shard_map/experts/pallas_call | solution.py:298
  102.5 1.2 collective-permute-start.16
  104.6 5.8 %experts.6 = (bf16[176,512]{1,0:T(8,128)(2,1)S(1)}, bf16[176,512]{1,0:T(8,128)(2,1)S(1)}, bf16[176,512]{1,0:T(8,128)(2,1)S(1)}, bf16[176,512]{1,0:T(8,128)(2,1)S(1)}) custom-call(s32[8]{0:T(128)S(1)} %copy-done.6, f32[1,2048]{1,0:T(1,128)S(1)} %constant_dynamic-update-slice_fusion.12.gain_ref, ...), custom_call_target="tpu_custom_call" | custom-call | tf_op jit(solution)/shard_map/experts/pallas_call | solution.py:298
  111.4 1.2 collective-permute-start.39
  112.6 5.8 %experts.7 = (bf16[176,512]{1,0:T(8,128)(2,1)S(1)}, bf16[176,512]{1,0:T(8,128)(2,1)S(1)}, bf16[176,512]{1,0:T(8,128)(2,1)S(1)}, bf16[176,512]{1,0:T(8,128)(2,1)S(1)}) custom-call(s32[8]{0:T(128)S(1)} %copy-done.6, f32[1,2048]{1,0:T(1,128)S(1)} %constant_dynamic-update-slice_fusion.12.gain_ref, ...), custom_call_target="tpu_custom_call" | custom-call | tf_op jit(solution)/shard_map/experts/pallas_call | solution.py:298
  118.5 1.1 collective-permute-start.41
  119.7 1.0 collective-permute-start.51
  121.7 1.3 collective-permute-start.19
  123.1 1.1 collective-permute-start.17
  124.3 1.7 %collective-permute-done.41 = bf16[176,512]{1,0:T(8,128)(2,1)S(1)} collective-permute-done((bf16[176,512]{1,0:T(8,128)(2,1)S(1)}, bf16[176,512]{1,0:T(8,128)(2,1)S(1)}, u32[]{:S(2)}, u32[]{:S(2)}) %collective-permute-start.41) | collective-permute-done | bytes 180256 | tf_op jit(solution)/shard_map/ppermute | solution.py:176
  125.9 1.1 collective-permute-start.28
  127.1 1.0 collective-permute-start.30
  128.1 1.7 %collective-permute-done.53 = bf16[176,512]{1,0:T(8,128)(2,1)S(1)} collective-permute-done((bf16[176,512]{1,0:T(8,128)(2,1)S(1)}, bf16[176,512]{1,0:T(8,128)(2,1)S(1)}, u32[]{:S(2)}, u32[]{:S(2)}) %collective-permute-start.53) | collective-permute-done | bytes 180256 | tf_op jit(solution)/shard_map/ppermute | solution.py:176
  129.8 1.1 collective-permute-start.40
  131.0 1.0 collective-permute-start.42
  132.0 1.0 collective-permute-start.52
  133.0 1.3 collective-permute-start.54
  134.5 1.4 collective-permute-start.31
  136.6 1.0 collective-permute-start.43
  137.6 2.2 %collective-permute-start.44 = (bf16[88,512]{1,0:T(8,128)(2,1)S(1)}, bf16[88,512]{1,0:T(8,128)(2,1)S(1)}, u32[]{:S(2)}, u32[]{:S(2)}) collective-permute-start(bf16[88,512]{1,0:T(8,128)(2,1)S(1)} %get-tuple-element.64), channel_id=1, source_target_pairs={{0,20},{4,16},{8,28},{12,24},{16,4},{20,0},{24,12},{28,8},{1,21},{... | collective-permute-start | bytes 270344 | tf_op jit(solution)/shard_map/ppermute | solution.py:173
  140.0 1.6 %collective-permute-start.55 = (bf16[88,512]{1,0:T(8,128)(2,1)S(1)}, bf16[88,512]{1,0:T(8,128)(2,1)S(1)}, u32[]{:S(2)}, u32[]{:S(2)}) collective-permute-start(bf16[88,512]{1,0:T(8,128)(2,1)S(1)} %get-tuple-element.67), channel_id=1, source_target_pairs={{0,24},{4,28},{8,16},{12,20},{16,8},{20,12},{24,0},{28,4},{1,25},{... | collective-permute-start | bytes 270344 | tf_op jit(solution)/shard_map/ppermute | solution.py:173
  141.6 3.6 %collective-permute-start.56 = (bf16[88,512]{1,0:T(8,128)(2,1)S(1)}, bf16[88,512]{1,0:T(8,128)(2,1)S(1)}, u32[]{:S(2)}, u32[]{:S(2)}) collective-permute-start(bf16[88,512]{1,0:T(8,128)(2,1)S(1)} %get-tuple-element.66), channel_id=1, source_target_pairs={{0,28},{4,24},{8,20},{12,16},{16,12},{20,8},{24,4},{28,0},{1,29},{... | collective-permute-start | bytes 270344 | tf_op jit(solution)/shard_map/ppermute | solution.py:173
  145.5 5.2 %collective-permute-done.43 = bf16[88,512]{1,0:T(8,128)(2,1)S(1)} collective-permute-done((bf16[88,512]{1,0:T(8,128)(2,1)S(1)}, bf16[88,512]{1,0:T(8,128)(2,1)S(1)}, u32[]{:S(2)}, u32[]{:S(2)}) %collective-permute-start.43) | collective-permute-done | bytes 90144 | tf_op jit(solution)/shard_map/ppermute | solution.py:173
  150.7 1.7 %collective-permute-done.44 = bf16[88,512]{1,0:T(8,128)(2,1)S(1)} collective-permute-done((bf16[88,512]{1,0:T(8,128)(2,1)S(1)}, bf16[88,512]{1,0:T(8,128)(2,1)S(1)}, u32[]{:S(2)}, u32[]{:S(2)}) %collective-permute-start.44) | collective-permute-done | bytes 90144 | tf_op jit(solution)/shard_map/ppermute | solution.py:173
  154.2 1.0 fusion.8
  (201 shorter events, 18.9 us)
Async XLA Ops:
  0.0 13.8 %copy-start.10 = (bf16[256,256]{1,0:T(8,128)(2,1)S(1)}, bf16[256,256]{1,0:T(8,128)(2,1)}, u32[]{:S(2)}) copy-start(bf16[256,256]{1,0:T(8,128)(2,1)} %param.13) | copy-start | bytes 393220
  0.0 13.9 %copy-start.14 = (f32[64]{0:T(128)S(1)}, f32[64]{0:T(128)}, u32[]{:S(2)}) copy-start(f32[64]{0:T(128)} %param.16) | copy-start | bytes 772
  0.0 14.7 %copy-start.12 = (s32[256,2]{0,1:T(2,128)S(1)}, s32[256,2]{0,1:T(2,128)}, u32[]{:S(2)}) copy-start(s32[256,2]{0,1:T(2,128)} %param.21) | copy-start | bytes 6148
  4.8 10.2 %collective-permute-start = (bf16[256,128]{1,0:T(8,128)(2,1)S(1)}, bf16[256,128]{1,0:T(8,128)(2,1)S(1)}, u32[]{:S(2)}, u32[]{:S(2)}) collective-permute-start(bf16[256,128]{1,0:T(8,128)(2,1)S(1)} %pad_maximum_fusion.11), channel_id=1, source_target_pairs={{0,8},{4,12},{8,0},{12,4},{16,24},{20,28},{24,16},{28,20},{1,9},{5... | collective-permute-start | bytes 196616 | tf_op jit(solution)/shard_map/ppermute | solution.py:173
  7.9 7.3 %collective-permute-start.1 = (bf16[256,128]{1,0:T(8,128)(2,1)S(1)}, bf16[256,128]{1,0:T(8,128)(2,1)S(1)}, u32[]{:S(2)}, u32[]{:S(2)}) collective-permute-start(bf16[256,128]{1,0:T(8,128)(2,1)S(1)} %pad_maximum_fusion.11), channel_id=1, source_target_pairs={{0,16},{4,20},{8,24},{12,28},{16,0},{20,4},{24,8},{28,12},{1,17},{... | collective-permute-start | bytes 196616 | tf_op jit(solution)/shard_map/ppermute | solution.py:173
  10.5 6.1 %collective-permute-start.2 = (bf16[256,128]{1,0:T(8,128)(2,1)S(1)}, bf16[256,128]{1,0:T(8,128)(2,1)S(1)}, u32[]{:S(2)}, u32[]{:S(2)}) collective-permute-start(bf16[256,128]{1,0:T(8,128)(2,1)S(1)} %pad_maximum_fusion.11), channel_id=1, source_target_pairs={{0,24},{4,28},{8,16},{12,20},{16,8},{20,12},{24,0},{28,4},{1,25},{... | collective-permute-start | bytes 196616 | tf_op jit(solution)/shard_map/ppermute | solution.py:173
  10.5 52.4 %collective-permute-start.8 = (f32[512]{0:T(512)S(1)}, f32[512]{0:T(512)S(1)}, u32[]{:S(2)}, u32[]{:S(2)}) collective-permute-start(f32[512]{0:T(512)S(1)} %copy-done.11), channel_id=1, source_target_pairs={{0,1},{1,0},{2,3},{3,2},{4,5},{5,4},{6,7},{7,6},{8,9},{9,8},{10,11... | collective-permute-start | bytes 6152 | tf_op jit(solution)/shard_map/ppermute | solution.py:176
  12.2 56.2 %collective-permute-start.9 = (f32[512]{0:T(512)S(1)}, f32[512]{0:T(512)S(1)}, u32[]{:S(2)}, u32[]{:S(2)}) collective-permute-start(f32[512]{0:T(512)S(1)} %copy-done.11), channel_id=1, source_target_pairs={{0,2},{1,3},{2,0},{3,1},{4,6},{5,7},{6,4},{7,5},{8,10},{9,11},{10,... | collective-permute-start | bytes 6152 | tf_op jit(solution)/shard_map/ppermute | solution.py:176
  16.7 2.1 %collective-permute-start.3 = (bf16[1024,128]{1,0:T(8,128)(2,1)S(1)}, bf16[1024,128]{1,0:T(8,128)(2,1)S(1)}, u32[]{:S(2)}, u32[]{:S(2)}) collective-permute-start(bf16[1024,128]{1,0:T(8,128)(2,1)S(1)} %pad_maximum_fusion.refs_0_), channel_id=1, source_target_pairs={{0,4},{4,0},{8,12},{12,8},{16,20},{20,16},{24,28},{28,24},{1,5},{5... | collective-permute-start | bytes 786440 | tf_op jit(solution)/shard_map/ppermute | solution.py:173
  17.1 26.8 %copy-start.7 = (bf16[256,512]{1,0:T(8,128)(2,1)S(1)}, bf16[256,512]{1,0:T(8,128)(2,1)}, u32[]{:S(2)}) copy-start(bf16[256,512]{1,0:T(8,128)(2,1)} %param.19) | copy-start | bytes 786436
  26.1 8.9 %collective-permute-start.4 = (bf16[256,512]{1,0:T(8,128)(2,1)}, bf16[256,512]{1,0:T(8,128)(2,1)S(1)}, u32[]{:S(2)}, u32[]{:S(2)}) collective-permute-start(bf16[256,512]{1,0:T(8,128)(2,1)} %get-tuple-element.26), channel_id=1, source_target_pairs={{0,1},{1,0},{2,3},{3,2},{4,5},{5,4},{6,7},{7,6},{8,9},{9,8},{10,11... | collective-permute-start | bytes 786440 | tf_op jit(solution)/shard_map/ppermute | solution.py:176
  27.8 9.9 %collective-permute-start.6 = (bf16[256,512]{1,0:T(8,128)(2,1)}, bf16[256,512]{1,0:T(8,128)(2,1)S(1)}, u32[]{:S(2)}, u32[]{:S(2)}) collective-permute-start(bf16[256,512]{1,0:T(8,128)(2,1)} %get-tuple-element.28), channel_id=1, source_target_pairs={{0,2},{1,3},{2,0},{3,1},{4,6},{5,7},{6,4},{7,5},{8,10},{9,11},{10,... | collective-permute-start | bytes 786440 | tf_op jit(solution)/shard_map/ppermute | solution.py:176
  36.0 5.1 %collective-permute-start.5 = (bf16[256,256]{1,0:T(8,128)(2,1)S(1)}, bf16[256,256]{1,0:T(8,128)(2,1)S(1)}, u32[]{:S(2)}, u32[]{:S(2)}) collective-permute-start(bf16[256,256]{1,0:T(8,128)(2,1)S(1)} %slice.444), channel_id=1, source_target_pairs={{0,2},{1,3},{2,0},{3,1},{4,6},{5,7},{6,4},{7,5},{8,10},{9,11},{10,... | collective-permute-start | bytes 393224 | tf_op jit(solution)/shard_map/ppermute | solution.py:176
  37.6 48.9 %copy-start.1 = (bf16[1,2048,1024]{2,1,0:T(8,128)(2,1)S(1)}, bf16[1,2048,1024]{2,1,0:T(8,128)(2,1)}, u32[]{:S(2)}) copy-start(bf16[1,2048,1024]{2,1,0:T(8,128)(2,1)} %refs_5_.7) | copy-start | bytes 12582916
  37.6 48.9 %copy-start.2 = (bf16[1,2048,1024]{2,1,0:T(8,128)(2,1)S(1)}, bf16[1,2048,1024]{2,1,0:T(8,128)(2,1)}, u32[]{:S(2)}) copy-start(bf16[1,2048,1024]{2,1,0:T(8,128)(2,1)} %refs_6_.7) | copy-start | bytes 12582916
  37.6 48.9 %copy-start.6 = (s32[8]{0:T(128)S(1)}, s32[8]{0:T(128)}, u32[]{:S(2)}) copy-start(s32[8]{0:T(128)} %stack.35.offs_ref) | copy-start | bytes 100
  38.8 5.0 %collective-permute-start.7 = (bf16[256,256]{1,0:T(8,128)(2,1)S(1)}, bf16[256,256]{1,0:T(8,128)(2,1)S(1)}, u32[]{:S(2)}, u32[]{:S(2)}) collective-permute-start(bf16[256,256]{1,0:T(8,128)(2,1)S(1)} %slice.443), channel_id=1, source_target_pairs={{0,1},{1,0},{2,3},{3,2},{4,5},{5,4},{6,7},{7,6},{8,9},{9,8},{10,11... | collective-permute-start | bytes 393224 | tf_op jit(solution)/shard_map/ppermute | solution.py:176
  44.4 2.0 %collective-permute-start.11 = (bf16[88,512]{1,0:T(8,128)(2,1)S(1)}, bf16[88,512]{1,0:T(8,128)(2,1)S(1)}, u32[]{:S(2)}, u32[]{:S(2)}) collective-permute-start(bf16[88,512]{1,0:T(8,128)(2,1)S(1)} %get-tuple-element.55), channel_id=1, source_target_pairs={{0,4},{4,0},{8,12},{12,8},{16,20},{20,16},{24,28},{28,24},{1,5},{5... | collective-permute-start | bytes 270344 | tf_op jit(solution)/shard_map/ppermute | solution.py:173
  44.5 5.6 %collective-permute-start.21 = (bf16[88,512]{1,0:T(8,128)(2,1)S(1)}, bf16[88,512]{1,0:T(8,128)(2,1)S(1)}, u32[]{:S(2)}, u32[]{:S(2)}) collective-permute-start(bf16[88,512]{1,0:T(8,128)(2,1)S(1)} %get-tuple-element.54), channel_id=1, source_target_pairs={{0,8},{4,12},{8,0},{12,4},{16,24},{20,28},{24,16},{28,20},{1,9},{5... | collective-permute-start | bytes 270344 | tf_op jit(solution)/shard_map/ppermute | solution.py:173
  44.6 16.0 %collective-permute-start.22 = (bf16[88,512]{1,0:T(8,128)(2,1)S(1)}, bf16[88,512]{1,0:T(8,128)(2,1)S(1)}, u32[]{:S(2)}, u32[]{:S(2)}) collective-permute-start(bf16[88,512]{1,0:T(8,128)(2,1)S(1)} %get-tuple-element.53), channel_id=1, source_target_pairs={{0,12},{4,8},{8,4},{12,0},{16,28},{20,24},{24,20},{28,16},{1,13},{... | collective-permute-start | bytes 270344 | tf_op jit(solution)/shard_map/ppermute | solution.py:173
  46.4 5.9 %collective-permute-start.33 = (bf16[88,512]{1,0:T(8,128)(2,1)S(1)}, bf16[88,512]{1,0:T(8,128)(2,1)S(1)}, u32[]{:S(2)}, u32[]{:S(2)}) collective-permute-start(bf16[88,512]{1,0:T(8,128)(2,1)S(1)} %get-tuple-element.52), channel_id=1, source_target_pairs={{0,16},{4,20},{8,24},{12,28},{16,0},{20,4},{24,8},{28,12},{1,17},{... | collective-permute-start | bytes 270344 | tf_op jit(solution)/shard_map/ppermute | solution.py:173
  50.1 12.7 %collective-permute-start.34 = (bf16[88,512]{1,0:T(8,128)(2,1)S(1)}, bf16[88,512]{1,0:T(8,128)(2,1)S(1)}, u32[]{:S(2)}, u32[]{:S(2)}) collective-permute-start(bf16[88,512]{1,0:T(8,128)(2,1)S(1)} %get-tuple-element.51), channel_id=1, source_target_pairs={{0,20},{4,16},{8,28},{12,24},{16,4},{20,0},{24,12},{28,8},{1,21},{... | collective-permute-start | bytes 270344 | tf_op jit(solution)/shard_map/ppermute | solution.py:173
  52.3 8.3 %collective-permute-start.45 = (bf16[88,512]{1,0:T(8,128)(2,1)S(1)}, bf16[88,512]{1,0:T(8,128)(2,1)S(1)}, u32[]{:S(2)}, u32[]{:S(2)}) collective-permute-start(bf16[88,512]{1,0:T(8,128)(2,1)S(1)} %get-tuple-element.50), channel_id=1, source_target_pairs={{0,24},{4,28},{8,16},{12,20},{16,8},{20,12},{24,0},{28,4},{1,25},{... | collective-permute-start | bytes 270344 | tf_op jit(solution)/shard_map/ppermute | solution.py:173
  60.6 6.3 %collective-permute-start.46 = (bf16[88,512]{1,0:T(8,128)(2,1)S(1)}, bf16[88,512]{1,0:T(8,128)(2,1)S(1)}, u32[]{:S(2)}, u32[]{:S(2)}) collective-permute-start(bf16[88,512]{1,0:T(8,128)(2,1)S(1)} %get-tuple-element.49), channel_id=1, source_target_pairs={{0,28},{4,24},{8,20},{12,16},{16,12},{20,8},{24,4},{28,0},{1,29},{... | collective-permute-start | bytes 270344 | tf_op jit(solution)/shard_map/ppermute | solution.py:173
  60.6 8.4 %collective-permute-start.13 = (bf16[176,512]{1,0:T(8,128)(2,1)S(1)}, bf16[176,512]{1,0:T(8,128)(2,1)S(1)}, u32[]{:S(2)}, u32[]{:S(2)}) collective-permute-start(bf16[176,512]{1,0:T(8,128)(2,1)S(1)} %pad_maximum_fusion.1.refs_0_), channel_id=1, source_target_pairs={{0,2},{1,3},{2,0},{3,1},{4,6},{5,7},{6,4},{7,5},{8,10},{9,11},{10,... | collective-permute-start | bytes 540680 | tf_op jit(solution)/shard_map/ppermute | solution.py:176
  62.8 8.2 %collective-permute-start.12 = (bf16[176,512]{1,0:T(8,128)(2,1)S(1)}, bf16[176,512]{1,0:T(8,128)(2,1)S(1)}, u32[]{:S(2)}, u32[]{:S(2)}) collective-permute-start(bf16[176,512]{1,0:T(8,128)(2,1)S(1)} %pad_maximum_fusion.1.refs_0_), channel_id=1, source_target_pairs={{0,1},{1,0},{2,3},{3,2},{4,5},{5,4},{6,7},{7,6},{8,9},{9,8},{10,11... | collective-permute-start | bytes 540680 | tf_op jit(solution)/shard_map/ppermute | solution.py:176
  62.9 8.2 %collective-permute-start.24 = (bf16[176,512]{1,0:T(8,128)(2,1)S(1)}, bf16[176,512]{1,0:T(8,128)(2,1)S(1)}, u32[]{:S(2)}, u32[]{:S(2)}) collective-permute-start(bf16[176,512]{1,0:T(8,128)(2,1)S(1)} %constant_dynamic-update-slice_fusion.refs_0_), channel_id=1, source_target_pairs={{0,2},{1,3},{2,0},{3,1},{4,6},{5,7},{6,4},{7,5},{8,10},{9,11},{10,... | collective-permute-start | bytes 540680 | tf_op jit(solution)/shard_map/ppermute | solution.py:176
  66.9 7.4 %collective-permute-start.23 = (bf16[176,512]{1,0:T(8,128)(2,1)S(1)}, bf16[176,512]{1,0:T(8,128)(2,1)S(1)}, u32[]{:S(2)}, u32[]{:S(2)}) collective-permute-start(bf16[176,512]{1,0:T(8,128)(2,1)S(1)} %constant_dynamic-update-slice_fusion.refs_0_), channel_id=1, source_target_pairs={{0,1},{1,0},{2,3},{3,2},{4,5},{5,4},{6,7},{7,6},{8,9},{9,8},{10,11... | collective-permute-start | bytes 540680 | tf_op jit(solution)/shard_map/ppermute | solution.py:176
  68.4 11.2 %collective-permute-start.36 = (bf16[176,512]{1,0:T(8,128)(2,1)S(1)}, bf16[176,512]{1,0:T(8,128)(2,1)S(1)}, u32[]{:S(2)}, u32[]{:S(2)}) collective-permute-start(bf16[176,512]{1,0:T(8,128)(2,1)S(1)} %constant_dynamic-update-slice_fusion.4.refs_0_), channel_id=1, source_target_pairs={{0,2},{1,3},{2,0},{3,1},{4,6},{5,7},{6,4},{7,5},{8,10},{9,11},{10,... | collective-permute-start | bytes 540680 | tf_op jit(solution)/shard_map/ppermute | solution.py:176
  69.0 11.6 %collective-permute-start.35 = (bf16[176,512]{1,0:T(8,128)(2,1)S(1)}, bf16[176,512]{1,0:T(8,128)(2,1)S(1)}, u32[]{:S(2)}, u32[]{:S(2)}) collective-permute-start(bf16[176,512]{1,0:T(8,128)(2,1)S(1)} %constant_dynamic-update-slice_fusion.4.refs_0_), channel_id=1, source_target_pairs={{0,1},{1,0},{2,3},{3,2},{4,5},{5,4},{6,7},{7,6},{8,9},{9,8},{10,11... | collective-permute-start | bytes 540680 | tf_op jit(solution)/shard_map/ppermute | solution.py:176
  71.0 10.8 %collective-permute-start.48 = (bf16[176,512]{1,0:T(8,128)(2,1)S(1)}, bf16[176,512]{1,0:T(8,128)(2,1)S(1)}, u32[]{:S(2)}, u32[]{:S(2)}) collective-permute-start(bf16[176,512]{1,0:T(8,128)(2,1)S(1)} %constant_dynamic-update-slice_fusion.8.refs_0_), channel_id=1, source_target_pairs={{0,2},{1,3},{2,0},{3,1},{4,6},{5,7},{6,4},{7,5},{8,10},{9,11},{10,... | collective-permute-start | bytes 540680 | tf_op jit(solution)/shard_map/ppermute | solution.py:176
  71.1 8.0 %collective-permute-start.10 = (f32[512]{0:T(512)S(1)}, f32[512]{0:T(512)S(1)}, u32[]{:S(2)}, u32[]{:S(2)}) collective-permute-start(f32[512]{0:T(512)S(1)} %copy-done.11), channel_id=1, source_target_pairs={{0,3},{1,2},{2,1},{3,0},{4,7},{5,6},{6,5},{7,4},{8,11},{9,10},{10,... | collective-permute-start | bytes 6152 | tf_op jit(solution)/shard_map/ppermute | solution.py:176
  74.4 8.9 %collective-permute-start.47 = (bf16[176,512]{1,0:T(8,128)(2,1)S(1)}, bf16[176,512]{1,0:T(8,128)(2,1)S(1)}, u32[]{:S(2)}, u32[]{:S(2)}) collective-permute-start(bf16[176,512]{1,0:T(8,128)(2,1)S(1)} %constant_dynamic-update-slice_fusion.8.refs_0_), channel_id=1, source_target_pairs={{0,1},{1,0},{2,3},{3,2},{4,5},{5,4},{6,7},{7,6},{8,9},{9,8},{10,11... | collective-permute-start | bytes 540680 | tf_op jit(solution)/shard_map/ppermute | solution.py:176
  79.1 5.5 %collective-permute-start.14 = (bf16[176,256]{1,0:T(8,128)(2,1)S(1)}, bf16[176,256]{1,0:T(8,128)(2,1)S(1)}, u32[]{:S(2)}, u32[]{:S(2)}) collective-permute-start(bf16[176,256]{1,0:T(8,128)(2,1)S(1)} %slice.319), channel_id=1, source_target_pairs={{0,1},{1,0},{2,3},{3,2},{4,5},{5,4},{6,7},{7,6},{8,9},{9,8},{10,11... | collective-permute-start | bytes 270344 | tf_op jit(solution)/shard_map/ppermute | solution.py:176
  79.6 6.0 %collective-permute-start.15 = (bf16[176,256]{1,0:T(8,128)(2,1)S(1)}, bf16[176,256]{1,0:T(8,128)(2,1)S(1)}, u32[]{:S(2)}, u32[]{:S(2)}) collective-permute-start(bf16[176,256]{1,0:T(8,128)(2,1)S(1)} %slice.320), channel_id=1, source_target_pairs={{0,2},{1,3},{2,0},{3,1},{4,6},{5,7},{6,4},{7,5},{8,10},{9,11},{10,... | collective-permute-start | bytes 270344 | tf_op jit(solution)/shard_map/ppermute | solution.py:176
  80.6 13.9 %collective-permute-start.25 = (bf16[176,256]{1,0:T(8,128)(2,1)S(1)}, bf16[176,256]{1,0:T(8,128)(2,1)S(1)}, u32[]{:S(2)}, u32[]{:S(2)}) collective-permute-start(bf16[176,256]{1,0:T(8,128)(2,1)S(1)} %slice.330), channel_id=1, source_target_pairs={{0,1},{1,0},{2,3},{3,2},{4,5},{5,4},{6,7},{7,6},{8,9},{9,8},{10,11... | collective-permute-start | bytes 270344 | tf_op jit(solution)/shard_map/ppermute | solution.py:176
  81.8 13.8 %collective-permute-start.26 = (bf16[176,256]{1,0:T(8,128)(2,1)S(1)}, bf16[176,256]{1,0:T(8,128)(2,1)S(1)}, u32[]{:S(2)}, u32[]{:S(2)}) collective-permute-start(bf16[176,256]{1,0:T(8,128)(2,1)S(1)} %slice.331), channel_id=1, source_target_pairs={{0,2},{1,3},{2,0},{3,1},{4,6},{5,7},{6,4},{7,5},{8,10},{9,11},{10,... | collective-permute-start | bytes 270344 | tf_op jit(solution)/shard_map/ppermute | solution.py:176
  83.2 19.3 %collective-permute-start.37 = (bf16[176,256]{1,0:T(8,128)(2,1)S(1)}, bf16[176,256]{1,0:T(8,128)(2,1)S(1)}, u32[]{:S(2)}, u32[]{:S(2)}) collective-permute-start(bf16[176,256]{1,0:T(8,128)(2,1)S(1)} %slice.341), channel_id=1, source_target_pairs={{0,1},{1,0},{2,3},{3,2},{4,5},{5,4},{6,7},{7,6},{8,9},{9,8},{10,11... | collective-permute-start | bytes 270344 | tf_op jit(solution)/shard_map/ppermute | solution.py:176
  84.6 19.1 %collective-permute-start.38 = (bf16[176,256]{1,0:T(8,128)(2,1)S(1)}, bf16[176,256]{1,0:T(8,128)(2,1)S(1)}, u32[]{:S(2)}, u32[]{:S(2)}) collective-permute-start(bf16[176,256]{1,0:T(8,128)(2,1)S(1)} %slice.342), channel_id=1, source_target_pairs={{0,2},{1,3},{2,0},{3,1},{4,6},{5,7},{6,4},{7,5},{8,10},{9,11},{10,... | collective-permute-start | bytes 270344 | tf_op jit(solution)/shard_map/ppermute | solution.py:176
  85.7 24.8 %collective-permute-start.49 = (bf16[176,256]{1,0:T(8,128)(2,1)S(1)}, bf16[176,256]{1,0:T(8,128)(2,1)S(1)}, u32[]{:S(2)}, u32[]{:S(2)}) collective-permute-start(bf16[176,256]{1,0:T(8,128)(2,1)S(1)} %slice.352), channel_id=1, source_target_pairs={{0,1},{1,0},{2,3},{3,2},{4,5},{5,4},{6,7},{7,6},{8,9},{9,8},{10,11... | collective-permute-start | bytes 270344 | tf_op jit(solution)/shard_map/ppermute | solution.py:176
  94.6 16.8 %collective-permute-start.50 = (bf16[176,256]{1,0:T(8,128)(2,1)S(1)}, bf16[176,256]{1,0:T(8,128)(2,1)S(1)}, u32[]{:S(2)}, u32[]{:S(2)}) collective-permute-start(bf16[176,256]{1,0:T(8,128)(2,1)S(1)} %slice.353), channel_id=1, source_target_pairs={{0,2},{1,3},{2,0},{3,1},{4,6},{5,7},{6,4},{7,5},{8,10},{9,11},{10,... | collective-permute-start | bytes 270344 | tf_op jit(solution)/shard_map/ppermute | solution.py:176
  95.5 22.9 %collective-permute-start.18 = (bf16[176,512]{1,0:T(8,128)(2,1)S(1)}, bf16[176,512]{1,0:T(8,128)(2,1)S(1)}, u32[]{:S(2)}, u32[]{:S(2)}) collective-permute-start(bf16[176,512]{1,0:T(8,128)(2,1)S(1)} %get-tuple-element.32), channel_id=1, source_target_pairs={{0,2},{1,3},{2,0},{3,1},{4,6},{5,7},{6,4},{7,5},{8,10},{9,11},{10,... | collective-permute-start | bytes 540680 | tf_op jit(solution)/shard_map/ppermute | solution.py:176
  102.5 17.1 %collective-permute-start.16 = (bf16[176,512]{1,0:T(8,128)(2,1)S(1)}, bf16[176,512]{1,0:T(8,128)(2,1)S(1)}, u32[]{:S(2)}, u32[]{:S(2)}) collective-permute-start(bf16[176,512]{1,0:T(8,128)(2,1)S(1)} %get-tuple-element.30), channel_id=1, source_target_pairs={{0,1},{1,0},{2,3},{3,2},{4,5},{5,4},{6,7},{7,6},{8,9},{9,8},{10,11... | collective-permute-start | bytes 540680 | tf_op jit(solution)/shard_map/ppermute | solution.py:176
  103.7 17.0 %collective-permute-start.27 = (bf16[176,512]{1,0:T(8,128)(2,1)S(1)}, bf16[176,512]{1,0:T(8,128)(2,1)S(1)}, u32[]{:S(2)}, u32[]{:S(2)}) collective-permute-start(bf16[176,512]{1,0:T(8,128)(2,1)S(1)} %get-tuple-element.34), channel_id=1, source_target_pairs={{0,1},{1,0},{2,3},{3,2},{4,5},{5,4},{6,7},{7,6},{8,9},{9,8},{10,11... | collective-permute-start | bytes 540680 | tf_op jit(solution)/shard_map/ppermute | solution.py:176
  110.5 11.3 %collective-permute-start.29 = (bf16[176,512]{1,0:T(8,128)(2,1)S(1)}, bf16[176,512]{1,0:T(8,128)(2,1)S(1)}, u32[]{:S(2)}, u32[]{:S(2)}) collective-permute-start(bf16[176,512]{1,0:T(8,128)(2,1)S(1)} %get-tuple-element.36), channel_id=1, source_target_pairs={{0,2},{1,3},{2,0},{3,1},{4,6},{5,7},{6,4},{7,5},{8,10},{9,11},{10,... | collective-permute-start | bytes 540680 | tf_op jit(solution)/shard_map/ppermute | solution.py:176
  111.4 11.7 %collective-permute-start.39 = (bf16[176,512]{1,0:T(8,128)(2,1)S(1)}, bf16[176,512]{1,0:T(8,128)(2,1)S(1)}, u32[]{:S(2)}, u32[]{:S(2)}) collective-permute-start(bf16[176,512]{1,0:T(8,128)(2,1)S(1)} %get-tuple-element.38), channel_id=1, source_target_pairs={{0,1},{1,0},{2,3},{3,2},{4,5},{5,4},{6,7},{7,6},{8,9},{9,8},{10,11... | collective-permute-start | bytes 540680 | tf_op jit(solution)/shard_map/ppermute | solution.py:176
  118.5 7.5 %collective-permute-start.41 = (bf16[176,512]{1,0:T(8,128)(2,1)S(1)}, bf16[176,512]{1,0:T(8,128)(2,1)S(1)}, u32[]{:S(2)}, u32[]{:S(2)}) collective-permute-start(bf16[176,512]{1,0:T(8,128)(2,1)S(1)} %get-tuple-element.40), channel_id=1, source_target_pairs={{0,2},{1,3},{2,0},{3,1},{4,6},{5,7},{6,4},{7,5},{8,10},{9,11},{10,... | collective-permute-start | bytes 540680 | tf_op jit(solution)/shard_map/ppermute | solution.py:176
  119.7 7.4 %collective-permute-start.51 = (bf16[176,512]{1,0:T(8,128)(2,1)S(1)}, bf16[176,512]{1,0:T(8,128)(2,1)S(1)}, u32[]{:S(2)}, u32[]{:S(2)}) collective-permute-start(bf16[176,512]{1,0:T(8,128)(2,1)S(1)} %get-tuple-element.42), channel_id=1, source_target_pairs={{0,1},{1,0},{2,3},{3,2},{4,5},{5,4},{6,7},{7,6},{8,9},{9,8},{10,11... | collective-permute-start | bytes 540680 | tf_op jit(solution)/shard_map/ppermute | solution.py:176
  120.7 9.1 %collective-permute-start.53 = (bf16[176,512]{1,0:T(8,128)(2,1)S(1)}, bf16[176,512]{1,0:T(8,128)(2,1)S(1)}, u32[]{:S(2)}, u32[]{:S(2)}) collective-permute-start(bf16[176,512]{1,0:T(8,128)(2,1)S(1)} %get-tuple-element.44), channel_id=1, source_target_pairs={{0,2},{1,3},{2,0},{3,1},{4,6},{5,7},{6,4},{7,5},{8,10},{9,11},{10,... | collective-permute-start | bytes 540680 | tf_op jit(solution)/shard_map/ppermute | solution.py:176
  121.7 9.2 %collective-permute-start.19 = (bf16[176,256]{1,0:T(8,128)(2,1)S(1)}, bf16[176,256]{1,0:T(8,128)(2,1)S(1)}, u32[]{:S(2)}, u32[]{:S(2)}) collective-permute-start(bf16[176,256]{1,0:T(8,128)(2,1)S(1)} %slice.451), channel_id=1, source_target_pairs={{0,1},{1,0},{2,3},{3,2},{4,5},{5,4},{6,7},{7,6},{8,9},{9,8},{10,11... | collective-permute-start | bytes 270344 | tf_op jit(solution)/shard_map/ppermute | solution.py:176
  123.1 8.9 %collective-permute-start.17 = (bf16[176,256]{1,0:T(8,128)(2,1)S(1)}, bf16[176,256]{1,0:T(8,128)(2,1)S(1)}, u32[]{:S(2)}, u32[]{:S(2)}) collective-permute-start(bf16[176,256]{1,0:T(8,128)(2,1)S(1)} %slice.452), channel_id=1, source_target_pairs={{0,2},{1,3},{2,0},{3,1},{4,6},{5,7},{6,4},{7,5},{8,10},{9,11},{10,... | collective-permute-start | bytes 270344 | tf_op jit(solution)/shard_map/ppermute | solution.py:176
  125.9 7.0 %collective-permute-start.28 = (bf16[176,256]{1,0:T(8,128)(2,1)S(1)}, bf16[176,256]{1,0:T(8,128)(2,1)S(1)}, u32[]{:S(2)}, u32[]{:S(2)}) collective-permute-start(bf16[176,256]{1,0:T(8,128)(2,1)S(1)} %slice.450), channel_id=1, source_target_pairs={{0,2},{1,3},{2,0},{3,1},{4,6},{5,7},{6,4},{7,5},{8,10},{9,11},{10,... | collective-permute-start | bytes 270344 | tf_op jit(solution)/shard_map/ppermute | solution.py:176
  127.1 7.3 %collective-permute-start.30 = (bf16[176,256]{1,0:T(8,128)(2,1)S(1)}, bf16[176,256]{1,0:T(8,128)(2,1)S(1)}, u32[]{:S(2)}, u32[]{:S(2)}) collective-permute-start(bf16[176,256]{1,0:T(8,128)(2,1)S(1)} %slice.449), channel_id=1, source_target_pairs={{0,1},{1,0},{2,3},{3,2},{4,5},{5,4},{6,7},{7,6},{8,9},{9,8},{10,11... | collective-permute-start | bytes 270344 | tf_op jit(solution)/shard_map/ppermute | solution.py:176
  129.8 4.7 %collective-permute-start.40 = (bf16[176,256]{1,0:T(8,128)(2,1)S(1)}, bf16[176,256]{1,0:T(8,128)(2,1)S(1)}, u32[]{:S(2)}, u32[]{:S(2)}) collective-permute-start(bf16[176,256]{1,0:T(8,128)(2,1)S(1)} %slice.448), channel_id=1, source_target_pairs={{0,2},{1,3},{2,0},{3,1},{4,6},{5,7},{6,4},{7,5},{8,10},{9,11},{10,... | collective-permute-start | bytes 270344 | tf_op jit(solution)/shard_map/ppermute | solution.py:176
  131.0 4.9 %collective-permute-start.42 = (bf16[176,256]{1,0:T(8,128)(2,1)S(1)}, bf16[176,256]{1,0:T(8,128)(2,1)S(1)}, u32[]{:S(2)}, u32[]{:S(2)}) collective-permute-start(bf16[176,256]{1,0:T(8,128)(2,1)S(1)} %slice.447), channel_id=1, source_target_pairs={{0,1},{1,0},{2,3},{3,2},{4,5},{5,4},{6,7},{7,6},{8,9},{9,8},{10,11... | collective-permute-start | bytes 270344 | tf_op jit(solution)/shard_map/ppermute | solution.py:176
  132.0 4.6 %collective-permute-start.52 = (bf16[176,256]{1,0:T(8,128)(2,1)S(1)}, bf16[176,256]{1,0:T(8,128)(2,1)S(1)}, u32[]{:S(2)}, u32[]{:S(2)}) collective-permute-start(bf16[176,256]{1,0:T(8,128)(2,1)S(1)} %slice.446), channel_id=1, source_target_pairs={{0,2},{1,3},{2,0},{3,1},{4,6},{5,7},{6,4},{7,5},{8,10},{9,11},{10,... | collective-permute-start | bytes 270344 | tf_op jit(solution)/shard_map/ppermute | solution.py:176
  133.0 4.6 %collective-permute-start.54 = (bf16[176,256]{1,0:T(8,128)(2,1)S(1)}, bf16[176,256]{1,0:T(8,128)(2,1)S(1)}, u32[]{:S(2)}, u32[]{:S(2)}) collective-permute-start(bf16[176,256]{1,0:T(8,128)(2,1)S(1)} %slice.445), channel_id=1, source_target_pairs={{0,1},{1,0},{2,3},{3,2},{4,5},{5,4},{6,7},{7,6},{8,9},{9,8},{10,11... | collective-permute-start | bytes 270344 | tf_op jit(solution)/shard_map/ppermute | solution.py:176
  134.3 19.6 %collective-permute-start.20 = (bf16[88,512]{1,0:T(8,128)(2,1)S(1)}, bf16[88,512]{1,0:T(8,128)(2,1)S(1)}, u32[]{:S(2)}, u32[]{:S(2)}) collective-permute-start(bf16[88,512]{1,0:T(8,128)(2,1)S(1)} %get-tuple-element.61), channel_id=1, source_target_pairs={{0,4},{4,0},{8,12},{12,8},{16,20},{20,16},{24,28},{28,24},{1,5},{5... | collective-permute-start | bytes 270344 | tf_op jit(solution)/shard_map/ppermute | solution.py:173
  134.5 5.6 %collective-permute-start.31 = (bf16[88,512]{1,0:T(8,128)(2,1)S(1)}, bf16[88,512]{1,0:T(8,128)(2,1)S(1)}, u32[]{:S(2)}, u32[]{:S(2)}) collective-permute-start(bf16[88,512]{1,0:T(8,128)(2,1)S(1)} %get-tuple-element.63), channel_id=1, source_target_pairs={{0,8},{4,12},{8,0},{12,4},{16,24},{20,28},{24,16},{28,20},{1,9},{5... | collective-permute-start | bytes 270344 | tf_op jit(solution)/shard_map/ppermute | solution.py:173
  135.9 5.7 %collective-permute-start.32 = (bf16[88,512]{1,0:T(8,128)(2,1)S(1)}, bf16[88,512]{1,0:T(8,128)(2,1)S(1)}, u32[]{:S(2)}, u32[]{:S(2)}) collective-permute-start(bf16[88,512]{1,0:T(8,128)(2,1)S(1)} %get-tuple-element.62), channel_id=1, source_target_pairs={{0,12},{4,8},{8,4},{12,0},{16,28},{20,24},{24,20},{28,16},{1,13},{... | collective-permute-start | bytes 270344 | tf_op jit(solution)/shard_map/ppermute | solution.py:173
  136.6 14.2 %collective-permute-start.43 = (bf16[88,512]{1,0:T(8,128)(2,1)S(1)}, bf16[88,512]{1,0:T(8,128)(2,1)S(1)}, u32[]{:S(2)}, u32[]{:S(2)}) collective-permute-start(bf16[88,512]{1,0:T(8,128)(2,1)S(1)} %get-tuple-element.65), channel_id=1, source_target_pairs={{0,16},{4,20},{8,24},{12,28},{16,0},{20,4},{24,8},{28,12},{1,17},{... | collective-permute-start | bytes 270344 | tf_op jit(solution)/shard_map/ppermute | solution.py:173
  137.6 14.8 %collective-permute-start.44 = (bf16[88,512]{1,0:T(8,128)(2,1)S(1)}, bf16[88,512]{1,0:T(8,128)(2,1)S(1)}, u32[]{:S(2)}, u32[]{:S(2)}) collective-permute-start(bf16[88,512]{1,0:T(8,128)(2,1)S(1)} %get-tuple-element.64), channel_id=1, source_target_pairs={{0,20},{4,16},{8,28},{12,24},{16,4},{20,0},{24,12},{28,8},{1,21},{... | collective-permute-start | bytes 270344 | tf_op jit(solution)/shard_map/ppermute | solution.py:173
  140.0 13.3 %collective-permute-start.55 = (bf16[88,512]{1,0:T(8,128)(2,1)S(1)}, bf16[88,512]{1,0:T(8,128)(2,1)S(1)}, u32[]{:S(2)}, u32[]{:S(2)}) collective-permute-start(bf16[88,512]{1,0:T(8,128)(2,1)S(1)} %get-tuple-element.67), channel_id=1, source_target_pairs={{0,24},{4,28},{8,16},{12,20},{16,8},{20,12},{24,0},{28,4},{1,25},{... | collective-permute-start | bytes 270344 | tf_op jit(solution)/shard_map/ppermute | solution.py:173
  141.6 11.7 %collective-permute-start.56 = (bf16[88,512]{1,0:T(8,128)(2,1)S(1)}, bf16[88,512]{1,0:T(8,128)(2,1)S(1)}, u32[]{:S(2)}, u32[]{:S(2)}) collective-permute-start(bf16[88,512]{1,0:T(8,128)(2,1)S(1)} %get-tuple-element.66), channel_id=1, source_target_pairs={{0,28},{4,24},{8,20},{12,16},{16,12},{20,8},{24,4},{28,0},{1,29},{... | collective-permute-start | bytes 270344 | tf_op jit(solution)/shard_map/ppermute | solution.py:173
  (8 other events, 48.7 us)
